TPU v7x, 256 devices: a whole 4x4x8 slice. The times are simulated.
256 devices in a mesh: sp: 64 (over z, x, core), tp: 4 (over y).
Axes of the slice: x: 4, y: 4, z: 8, core: 2. Of those that a mesh axis runs over, the one named last changes fastest.
Arguments:
- hidden_in: bfloat16 [16384, 2048], P('sp'), may hold values from -6 to 6
- cotangent: bfloat16 [16384, 2048], P('sp'), may hold values from -16 to 16
- routes: int32 [16384, 2], P('sp'), may hold values from 0 to 63, all different within a row; in each aligned block of 256 rows (0 to 255, 256 to 511, ...) at most 12 rows name the same one
- routing_weights: float32 [16384, 2], P('sp'), may hold values from 0.1 to 1
- w_gate: bfloat16 [64, 2048, 1024], P('sp', None, 'tp'), may hold values from -0.125 to 0.125
- w_up: bfloat16 [64, 2048, 1024], P('sp', None, 'tp'), may hold values from -0.125 to 0.125
- w_down: bfloat16 [64, 1024, 2048], P('sp', 'tp'), may hold values from -0.1875 to 0.1875
- b_gate: bfloat16 [16384, 1024], P('sp', 'tp'), may hold values from -6 to 6
- c_gate: bfloat16 [16384, 1024], P('sp', 'tp'), may hold values from -6 to 6
- x_in: bfloat16 [16384, 1024], P('sp', 'tp'), may hold values from -6 to 6
- taps: bfloat16 [3, 1024], P(None, 'tp'), may hold values from -3 to 3
- w_out: bfloat16 [2048, 1024], P(None, 'tp'), may hold values from -0.1875 to 0.1875
Outputs:
- grad_gate: bfloat16 [64, 2048, 1024], P('sp', None, 'tp')
- grad_up: bfloat16 [64, 2048, 1024], P('sp', None, 'tp')
- grad_down: bfloat16 [64, 1024, 2048], P('sp', 'tp')
- out_proj_grad: float32 [2048, 1024], P('sp', 'tp')
- residual_grad: bfloat16 [16384, 2048], P('sp', 'tp')
- grad_b: bfloat16 [16384, 1024], P('sp', 'tp')
- grad_c: bfloat16 [16384, 1024], P('sp', 'tp')
- grad_x: bfloat16 [16384, 1024], P('sp', 'tp')
Inputs may be any that keep to these rules, and one draw needn't show every extreme that they name: `routes`: each row names 2 different experts. Among the rows of one index of sp no expert is named more than 12 times, a bound that some block reaches in some of them.
All inputs are finite; a program needn't handle non-finite values.
Results may differ from a plain program's by a relative error of at most 0.01.
Values may be sent and summed in bfloat16 or wider, within the bound.
A program may use at most 64 MiB of HBM per device.

v0:
```python
import jax
import jax.numpy as jnp
from jax import lax
from jax.sharding import PartitionSpec as P


def in_one_piece(arrays, axis, split_dim, concat_dim, along):
    widths = [a.shape[along] for a in arrays]
    both = jnp.concatenate(arrays, axis=along)
    whole = lax.all_to_all(both, axis, split_axis=split_dim, concat_axis=concat_dim, tiled=True)
    return tuple(jnp.split(whole, [sum(widths[:k]) for k in range(1, len(widths))], axis=along))


def sent_together(arrays, axis, dim, along):
    ends, at = ([], 0)
    for a in arrays[:-1]:
        at += a.shape[along]
        ends.append(at)
    both = jnp.concatenate(arrays, axis=along)
    return tuple(jnp.split(lax.all_gather(both, axis, axis=dim, tiled=True), ends, axis=along))


def cut_along(x, dim, devices):
    before, after = (x.shape[:dim], x.shape[dim + 1 :])
    return jnp.moveaxis(x.reshape(*before, devices, -1, *after), dim, 0)


def summed_on_arrival(x, axis, dim):
    blocks = cut_along(x, dim, lax.axis_size(axis))
    arrived = lax.all_to_all(blocks, axis, split_axis=0, concat_axis=0, tiled=True)
    return arrived.astype(jnp.float32).sum(axis=0)


def laid_out(blocks, dim):
    lengths = list(blocks.shape[1:])
    lengths[dim] *= blocks.shape[0]
    return jnp.moveaxis(blocks, 0, dim).reshape(lengths)


def copy_for_each(x, axis):
    copies = jnp.broadcast_to(x, (lax.axis_size(axis), *x.shape))
    return lax.all_to_all(copies, axis, split_axis=0, concat_axis=0, tiled=True)


def gathered_copies(x, axis, dim):
    return laid_out(copy_for_each(x, axis), dim)


def from_behind(x, axis, by):
    devices = lax.axis_size(axis)
    pairs = [(i, i + by) for i in range(devices) if 0 <= i + by < devices]
    return lax.ppermute(x, axis, pairs)


def per_device(
    hidden_in,
    cotangent,
    routes,
    routing_weights,
    w_gate,
    w_up,
    w_down,
    b_gate,
    c_gate,
    x_in,
    taps,
    w_out,
):
    tok_rows, model_width = hidden_in.shape
    top_k = routes.shape[1]
    local_experts = w_gate.shape[0]
    sp_size = lax.axis_size("sp")
    tp_size = lax.axis_size("tp")
    experts = local_experts * sp_size
    capacity = 3 * tok_rows * top_k // (2 * experts)
    slot_count = tok_rows * top_k
    feature_share = model_width // tp_size
    share_offset = lax.axis_index("tp") * feature_share
    flat_ids = routes.reshape(-1)
    onehot = (flat_ids[:, None] == jnp.arange(experts, dtype=jnp.int32)[None, :]).astype(jnp.int32)
    before = jnp.cumsum(onehot, axis=0) - onehot
    position = jnp.sum(before * onehot, axis=1)
    target = flat_ids * capacity + position
    source = (
        jnp.full((experts * capacity,), slot_count, jnp.int32)
        .at[target]
        .set(jnp.arange(slot_count, dtype=jnp.int32))
    )
    filled = source < slot_count
    clipped = jnp.minimum(source, slot_count - 1)
    token_of = clipped // top_k
    weight_of = jnp.where(filled, routing_weights.reshape(-1)[clipped], 0.0)
    rows_src = lax.dynamic_slice_in_dim(hidden_in, share_offset, feature_share, 1)
    cot_src = lax.dynamic_slice_in_dim(cotangent, share_offset, feature_share, 1)
    send_rows = jnp.where(filled[:, None], rows_src[token_of], jnp.zeros((), jnp.bfloat16))
    send_rows = send_rows.reshape(experts, capacity, -1)
    send_cot = (weight_of[:, None] * cot_src[token_of].astype(jnp.float32)).astype(jnp.bfloat16)
    send_cot = send_cot.reshape(experts, capacity, -1)
    part_rows, part_cot = in_one_piece((send_rows, send_cot), "sp", 0, 1, 2)
    rows_h, rows_s = sent_together((part_rows, part_cot), "tp", 2, 0)
    pre_gate = jnp.einsum("erd,edf->erf", rows_h, w_gate, preferred_element_type=jnp.float32)
    pre_up = jnp.einsum("erd,edf->erf", rows_h, w_up, preferred_element_type=jnp.float32)
    sigma = jax.nn.sigmoid(pre_gate)
    silu_gate = pre_gate * sigma
    hid = (silu_gate * pre_up).astype(jnp.bfloat16)
    d_hid = jnp.einsum("erd,efd->erf", rows_s, w_down, preferred_element_type=jnp.float32)
    d_up = (d_hid * silu_gate).astype(jnp.bfloat16)
    d_pre = (d_hid * pre_up * sigma * (1.0 + pre_gate * (1.0 - sigma))).astype(jnp.bfloat16)
    grad_down = jnp.einsum("erf,erd->efd", hid, rows_s, preferred_element_type=jnp.float32).astype(
        jnp.bfloat16
    )
    grad_gate = jnp.einsum(
        "erd,erf->edf", rows_h, d_pre, preferred_element_type=jnp.float32
    ).astype(jnp.bfloat16)
    grad_up = jnp.einsum("erd,erf->edf", rows_h, d_up, preferred_element_type=jnp.float32).astype(
        jnp.bfloat16
    )
    partial_grad = jnp.einsum("erf,edf->erd", d_pre, w_gate, preferred_element_type=jnp.float32)
    partial_grad = partial_grad + jnp.einsum(
        "erf,edf->erd", d_up, w_up, preferred_element_type=jnp.float32
    )
    partial_low = partial_grad.astype(jnp.bfloat16)
    shared_rows = summed_on_arrival(partial_low, "tp", 2).astype(jnp.bfloat16)
    back = lax.all_to_all(shared_rows, "sp", split_axis=1, concat_axis=0, tiled=True)
    back_flat = back.reshape(experts * capacity, feature_share)
    per_token = back_flat[target].astype(jnp.float32).reshape(tok_rows, top_k, feature_share)
    own_cot = lax.dynamic_slice_in_dim(cotangent, share_offset, feature_share, 1).astype(
        jnp.float32
    )
    residual_grad = (own_cot + jnp.sum(per_token, axis=1)).astype(jnp.bfloat16)
    full_grad = gathered_copies(residual_grad, "tp", 1)
    taps_f = taps.astype(jnp.float32)
    gated = c_gate.astype(jnp.float32) * x_in.astype(jnp.float32)
    earlier = from_behind(gated[tok_rows - 2 :], "sp", 1)
    padded = jnp.concatenate([earlier, gated], axis=0)
    conv = (
        taps_f[0] * padded[0:tok_rows]
        + taps_f[1] * padded[1 : tok_rows + 1]
        + taps_f[2] * padded[2 : tok_rows + 2]
    )
    b_f = b_gate.astype(jnp.float32)
    y_short = (b_f * conv).astype(jnp.bfloat16)
    d_y = jnp.dot(full_grad, w_out, preferred_element_type=jnp.float32)
    grad_b = (d_y * conv).astype(jnp.bfloat16)
    d_conv = b_f * d_y
    following = from_behind(d_conv[0:2], "sp", -1)
    later = jnp.concatenate([d_conv, following], axis=0)
    d_v = (
        taps_f[2] * later[0:tok_rows]
        + taps_f[1] * later[1 : tok_rows + 1]
        + taps_f[0] * later[2 : tok_rows + 2]
    )
    grad_c = (d_v * x_in.astype(jnp.float32)).astype(jnp.bfloat16)
    grad_x = (d_v * c_gate.astype(jnp.float32)).astype(jnp.bfloat16)
    out_proj_grad = summed_on_arrival(
        jnp.einsum("td,tc->dc", full_grad, y_short, preferred_element_type=jnp.float32).astype(
            jnp.bfloat16
        ),
        "sp",
        0,
    )
    return (grad_gate, grad_up, grad_down, out_proj_grad, residual_grad, grad_b, grad_c, grad_x)


def solution(mesh):
    return jax.shard_map(
        per_device,
        mesh=mesh,
        in_specs=(
            P("sp", None),
            P("sp", None),
            P("sp", None),
            P("sp", None),
            P("sp", None, "tp"),
            P("sp", None, "tp"),
            P("sp", "tp", None),
            P("sp", "tp"),
            P("sp", "tp"),
            P("sp", "tp"),
            P(None, "tp"),
            P(None, "tp"),
        ),
        out_specs=(
            P("sp", None, "tp"),
            P("sp", None, "tp"),
            P("sp", "tp", None),
            P("sp", "tp"),
            P("sp", "tp"),
            P("sp", "tp"),
            P("sp", "tp"),
            P("sp", "tp"),
        ),
        check_vma=False,
    )
```

profile of v0, /device:TPU:1, one launch (start us, length us, event | category | flops | bytes accessed | tf_op | source)
XLA Modules:
  0.0 338.7 jit_solution(15847824969472595862)
XLA Ops:
  11.0 2.4 scatter_custom_fusion
  14.5 3.3 gather_fusion.2
  19.4 5.0 %gather_fusion.1 = f32[768]{0:T(1024)S(1)} fusion(f32[512]{0:T(512)S(1)} %reshape.169, s32[1024]{0:T(1024)S(1)} %get-tuple-element.24), kind=kCustom, calls=%fused_computation.1 | custom fusion | bytes 9216 | tf_op jit(solution)/shard_map/gather | solution.py:92
  25.5 3.3 gather_fusion
  32.8 62.5 %all_to_all.36 = bf16[64,12,1024]{2,1,0:T(8,128)(2,1)S(1)} all-to-all(bf16[64,12,1024]{2,1,0:T(8,128)(2,1)S(1)} %pad_maximum_fusion), channel_id=1, replica_groups=mesh['sp'=64,'tp'=4] {'sp'}, dimensions={0} | all-to-all | bytes 3145728 | tf_op jit(solution)/shard_map/all_to_all | solution.py:10
  99.4 66.0 %all-gather.2.cloned.1.call-done = bf16[2,768,2048]{2,1,0:T(8,128)(2,1)} async-done(((bf16[2,768,512]{2,1,0:T(8,128)(2,1)}), bf16[2,768,2048]{2,1,0:T(8,128)(2,1)}) %all-gather.2.cloned.1.call-update) | async-done | bytes 6291472 | tf_op jit(solution)/shard_map/all_gather | solution.py:20
  165.3 3.0 fusion.6
  172.8 2.8 add_convert_fusion
  175.6 4.8 %reshape.175 = bf16[1,768,4,512]{3,2,1,0:T(4,128)(2,1)S(1)} reshape(bf16[768,2048]{1,0:T(8,128)(2,1)} %add_convert_fusion) | data formatting | bytes 6291456 | tf_op jit(solution)/shard_map/reshape | solution.py:25
  181.1 39.7 %all_to_all.37 = bf16[4,1,768,512]{3,2,1,0:T(8,128)(2,1)S(1)} all-to-all(bf16[4,1,768,512]{3,2,1,0:T(8,128)(2,1)S(1)} %bitcast.84), channel_id=1, replica_groups=mesh['sp'=64,'tp'=4] {'tp'}, dimensions={0} | all-to-all | bytes 6291456 | tf_op jit(solution)/shard_map/all_to_all | solution.py:30
  222.4 2.3 copy.49
  225.2 5.4 %reduce.4 = bf16[768,512]{1,0:T(8,128)(2,1)S(1)} reduce(bf16[768,1,512]{2,1,0:T(2,128)(2,1)S(1)} %bitcast.87, bf16[]{:T(256)} %broadcast.112), dimensions={1}, to_apply=%bitcast.82.reduce_sub_computation | reduce | bytes 1572866
  231.9 12.0 %all-to-all-start.2 = ((bf16[64,2,3072]{2,1,0:T(2,128)(2,1)}), bf16[64,2,3072]{2,1,0:T(2,128)(2,1)S(1)}, u32[]{:S(2)}, u32[]{:S(2)}) async-start(bf16[64,2,3072]{2,1,0:T(2,128)(2,1)} %reshape.227), calls=%async_computation.2 | async-start | bytes 1572864 | tf_op jit(solution)/shard_map/all_to_all | solution.py:124
  243.9 23.0 %all-to-all-done.2 = bf16[64,2,3072]{2,1,0:T(2,128)(2,1)S(1)} async-done(((bf16[64,2,3072]{2,1,0:T(2,128)(2,1)}), bf16[64,2,3072]{2,1,0:T(2,128)(2,1)S(1)}, u32[]{:S(2)}, u32[]{:S(2)}) %all-to-all-start.2) | async-done | bytes 786464 | tf_op jit(solution)/shard_map/all_to_all | solution.py:124
  273.9 3.8 %all-to-all-start.3 = ((bf16[4,256,512]{1,2,0:T(8,128)(2,1)}), bf16[4,256,512]{1,2,0:T(8,128)(2,1)S(1)}, u32[]{:S(2)}, u32[]{:S(2)}) async-start(bf16[4,256,512]{1,2,0:T(8,128)(2,1)} %broadcast_in_dim.39), calls=%async_computation.3 | async-start | bytes 2097152 | tf_op jit(solution)/shard_map/all_to_all | solution.py:42
  277.7 3.7 %collective-permute-start = (f32[2,256]{1,0:T(2,128)S(1)}, f32[2,256]{1,0:T(2,128)S(1)}, u32[]{:S(2)}, u32[]{:S(2)}) collective-permute-start(f32[2,256]{1,0:T(2,128)S(1)} %slice.57), channel_id=1, source_target_pairs={{0,4},{4,8},{8,12},{12,16},{16,20},{20,24},{24,28},{28,32},{32,36}... | collective-permute-start | bytes 6152 | tf_op jit(solution)/shard_map/ppermute | solution.py:52
  282.1 9.7 %all-to-all-done.3 = bf16[4,256,512]{1,2,0:T(8,128)(2,1)S(1)} async-done(((bf16[4,256,512]{1,2,0:T(8,128)(2,1)}), bf16[4,256,512]{1,2,0:T(8,128)(2,1)S(1)}, u32[]{:S(2)}, u32[]{:S(2)}) %all-to-all-start.3) | async-done | bytes 1048608 | tf_op jit(solution)/shard_map/all_to_all | solution.py:42
  293.9 2.3 convolution_convert_fusion
  296.2 6.6 %all-to-all-start.4 = ((bf16[64,32,256]{2,1,0:T(8,128)(2,1)}), bf16[64,32,256]{2,1,0:T(8,128)(2,1)S(1)}, u32[]{:S(2)}, u32[]{:S(2)}) async-start(bf16[64,32,256]{2,1,0:T(8,128)(2,1)} %bitcast.18), calls=%async_computation.4 | async-start | bytes 2097152 | tf_op jit(solution)/shard_map/all_to_all | solution.py:30
  302.9 4.0 %fusion.3 = bf16[1,2048,256]{2,1,0:T(8,128)(2,1)} fusion(bf16[768,256]{1,0:T(8,128)(2,1)S(1)} %get-tuple-element.15, bf16[2,768,2048]{2,1,0:T(8,128)(2,1)} %all-gather.2.cloned.1.call-done), kind=kOutput, calls=%fused_computation.15 | convolution fusion | flops 805830656 | bytes 4587520 | tf_op jit(solution)/shard_map/erd,erf->edf/dot_general | solution.py:112
  306.9 4.0 %fusion.5 = bf16[1,256,2048]{2,1,0:T(8,128)(2,1)} fusion(bf16[2,768,2048]{2,1,0:T(8,128)(2,1)} %all-gather.2.cloned.1.call-done, f32[768,256]{1,0:T(8,128)S(1)} %copy-done.19, f32[768,256]{1,0:T(8,128)S(1)} %copy-done.17), kind=kOutput, calls=%fused_computation.17 | convolution fusion | flops 807010304 | bytes 5767168 | tf_op jit(solution)/shard_map/erf,erd->efd/dot_general | solution.py:109
  310.9 2.5 collective-permute-start.1
  313.4 4.0 %fusion.4 = bf16[1,2048,256]{2,1,0:T(8,128)(2,1)} fusion(bf16[768,256]{1,0:T(8,128)(2,1)S(1)} %copy-done.11, bf16[2,768,2048]{2,1,0:T(8,128)(2,1)} %all-gather.2.cloned.1.call-done), kind=kOutput, calls=%fused_computation.16 | convolution fusion | flops 805830656 | bytes 4587520 | tf_op jit(solution)/shard_map/erd,erf->edf/dot_general | solution.py:115
  318.9 12.2 %all-to-all-done.4 = bf16[64,32,256]{2,1,0:T(8,128)(2,1)S(1)} async-done(((bf16[64,32,256]{2,1,0:T(8,128)(2,1)}), bf16[64,32,256]{2,1,0:T(8,128)(2,1)S(1)}, u32[]{:S(2)}, u32[]{:S(2)}) %all-to-all-start.4) | async-done | bytes 1048608 | tf_op jit(solution)/shard_map/all_to_all | solution.py:30
  (99 shorter events, 35.7 us)
Async XLA Ops:
  7.2 158.2 %copy-start = (bf16[1,2048,256]{2,1,0:T(8,128)(2,1)S(1)}, bf16[1,2048,256]{2,1,0:T(8,128)(2,1)}, u32[]{:S(2)}) copy-start(bf16[1,2048,256]{2,1,0:T(8,128)(2,1)} %param.16) | copy-start | bytes 3145732
  7.2 158.2 %all-gather.2.cloned.1.call-start = ((), (), s32[]{:S(2)}) async-start(), calls=%async_computation.5 | async-start | bytes 7864320 | tf_op jit(solution)/shard_map/all_gather | solution.py:20
  14.5 4.6 %copy-start.13 = (f32[256,2]{0,1:T(2,128)S(1)}, f32[256,2]{0,1:T(2,128)}, u32[]{:S(2)}) copy-start(f32[256,2]{0,1:T(2,128)} %param.15) | copy-start | bytes 6148
  31.0 1.2 copy-start.2
  99.4 69.0 %copy-start.5 = (bf16[1,2048,256]{2,1,0:T(8,128)(2,1)S(1)}, bf16[1,2048,256]{2,1,0:T(8,128)(2,1)}, u32[]{:S(2)}) copy-start(bf16[1,2048,256]{2,1,0:T(8,128)(2,1)} %param.17) | copy-start | bytes 3145732
  165.3 3.7 %copy-start.14 = (bf16[2,768,2048]{2,1,0:T(8,128)(2,1)S(1)}, bf16[2,768,2048]{2,1,0:T(8,128)(2,1)}, u32[]{:S(2)}) copy-start(bf16[2,768,2048]{2,1,0:T(8,128)(2,1)} %all-gather.2.cloned.1.call-done) | copy-start | bytes 18874372
  169.1 1.5 copy-start.15
  170.6 1.2 copy-start.18
  231.9 35.0 %all-to-all-start.2 = ((bf16[64,2,3072]{2,1,0:T(2,128)(2,1)}), bf16[64,2,3072]{2,1,0:T(2,128)(2,1)S(1)}, u32[]{:S(2)}, u32[]{:S(2)}) async-start(bf16[64,2,3072]{2,1,0:T(2,128)(2,1)} %reshape.227), calls=%async_computation.2 | async-start | bytes 1572864 | tf_op jit(solution)/shard_map/all_to_all | solution.py:124
  270.3 7.3 %copy-start.6 = (bf16[256,256]{1,0:T(8,128)(2,1)S(1)}, bf16[256,256]{1,0:T(8,128)(2,1)}, u32[]{:S(2)}) copy-start(bf16[256,256]{1,0:T(8,128)(2,1)} %param.20) | copy-start | bytes 393220
  270.4 7.3 %copy-start.8 = (bf16[256,256]{1,0:T(8,128)(2,1)S(1)}, bf16[256,256]{1,0:T(8,128)(2,1)}, u32[]{:S(2)}) copy-start(bf16[256,256]{1,0:T(8,128)(2,1)} %param.21) | copy-start | bytes 393220
  271.6 9.8 %copy-start.12 = (bf16[3,256]{1,0:T(4,128)(2,1)S(1)}, bf16[3,256]{1,0:T(4,128)(2,1)}, u32[]{:S(2)}) copy-start(bf16[3,256]{1,0:T(4,128)(2,1)} %param.22) | copy-start | bytes 4612
  272.7 21.2 %copy-start.4 = (bf16[256,512]{1,0:T(8,128)(2,1)}, bf16[256,512]{1,0:T(8,128)(2,1)S(1)}, u32[]{:S(2)}) copy-start(bf16[256,512]{1,0:T(8,128)(2,1)S(1)} %add_convert_fusion.1) | copy-start | bytes 786436
  272.7 19.2 %copy-start.3 = (bf16[2048,256]{1,0:T(8,128)(2,1)S(1)}, bf16[2048,256]{1,0:T(8,128)(2,1)}, u32[]{:S(2)}) copy-start(bf16[2048,256]{1,0:T(8,128)(2,1)} %param.23) | copy-start | bytes 3145732
  273.9 18.0 %all-to-all-start.3 = ((bf16[4,256,512]{1,2,0:T(8,128)(2,1)}), bf16[4,256,512]{1,2,0:T(8,128)(2,1)S(1)}, u32[]{:S(2)}, u32[]{:S(2)}) async-start(bf16[4,256,512]{1,2,0:T(8,128)(2,1)} %broadcast_in_dim.39), calls=%async_computation.3 | async-start | bytes 2097152 | tf_op jit(solution)/shard_map/all_to_all | solution.py:42
  277.7 4.4 %collective-permute-start = (f32[2,256]{1,0:T(2,128)S(1)}, f32[2,256]{1,0:T(2,128)S(1)}, u32[]{:S(2)}, u32[]{:S(2)}) collective-permute-start(f32[2,256]{1,0:T(2,128)S(1)} %slice.57), channel_id=1, source_target_pairs={{0,4},{4,8},{8,12},{12,16},{16,20},{20,24},{24,28},{28,32},{32,36}... | collective-permute-start | bytes 6152 | tf_op jit(solution)/shard_map/ppermute | solution.py:52
  296.2 34.8 %all-to-all-start.4 = ((bf16[64,32,256]{2,1,0:T(8,128)(2,1)}), bf16[64,32,256]{2,1,0:T(8,128)(2,1)S(1)}, u32[]{:S(2)}, u32[]{:S(2)}) async-start(bf16[64,32,256]{2,1,0:T(8,128)(2,1)} %bitcast.18), calls=%async_computation.4 | async-start | bytes 2097152 | tf_op jit(solution)/shard_map/all_to_all | solution.py:30
  302.9 4.0 %copy-start.17 = (f32[768,256]{1,0:T(8,128)S(1)}, f32[768,256]{1,0:T(8,128)}, u32[]{:S(2)}) copy-start(f32[768,256]{1,0:T(8,128)} %copy-done.16) | copy-start | bytes 2359300
  302.9 4.0 %copy-start.19 = (f32[768,256]{1,0:T(8,128)S(1)}, f32[768,256]{1,0:T(8,128)}, u32[]{:S(2)}) copy-start(f32[768,256]{1,0:T(8,128)} %copy-done.18) | copy-start | bytes 2359300
  306.9 6.5 %copy-start.11 = (bf16[768,256]{1,0:T(8,128)(2,1)S(1)}, bf16[768,256]{1,0:T(8,128)(2,1)}, u32[]{:S(2)}) copy-start(bf16[768,256]{1,0:T(8,128)(2,1)} %copy-done.10) | copy-start | bytes 1179652
  310.9 6.5 %copy-start.7 = (bf16[256,256]{1,0:T(8,128)(2,1)S(1)}, bf16[256,256]{1,0:T(8,128)(2,1)}, u32[]{:S(2)}) copy-start(bf16[256,256]{1,0:T(8,128)(2,1)} %param.20) | copy-start | bytes 393220
  310.9 7.3 %copy-start.9 = (bf16[256,256]{1,0:T(8,128)(2,1)S(1)}, bf16[256,256]{1,0:T(8,128)(2,1)}, u32[]{:S(2)}) copy-start(bf16[256,256]{1,0:T(8,128)(2,1)} %param.21) | copy-start | bytes 393220
  310.9 6.5 %collective-permute-start.1 = (f32[2,256]{1,0:T(2,128)S(1)}, f32[2,256]{1,0:T(2,128)S(1)}, u32[]{:S(2)}, u32[]{:S(2)}) collective-permute-start(f32[2,256]{1,0:T(2,128)S(1)} %slice.62), channel_id=1, source_target_pairs={{4,0},{8,4},{12,8},{16,12},{20,16},{24,20},{28,24},{32,28},{36,32}... | collective-permute-start | bytes 6152 | tf_op jit(solution)/shard_map/ppermute | solution.py:52
  313.4 18.4 %copy-start.1 = (bf16[1,2048,256]{2,1,0:T(8,128)(2,1)S(1)}, bf16[1,2048,256]{2,1,0:T(8,128)(2,1)}, u32[]{:S(2)}) copy-start(bf16[1,2048,256]{2,1,0:T(8,128)(2,1)} %param.16) | copy-start | bytes 3145732
  (2 other events, 2.0 us)
Sparse Core Ops, SparseCore 0:
  99.5 65.8 all-gather.1
where the time goes:
time: 340 us; the launch traced here: 339 us
  waiting for transfers between devices  112 us (33%)
  blocking collectives  102 us (30%)
  local copies, waits for them, and re-layouts  40.7 us (12%)
  starting transfers between devices  28.6 us (8%)
  matrix products  25.4 us (7%)
  other arithmetic  15.7 us (5%)
  between operations  14.6 us (4%)
    all_gather x1, waiting for transfers between devices, sent_together(): lax.all_gather(both, axis, axis=dim, tiled=True)  66 us
    all_to_all x1, blocking collectives, in_one_piece(): lax.all_to_all(both, axis, split_axis=split_dim, concat_axis=concat_dim,...  62.5 us
    all_to_all x1, blocking collectives, summed_on_arrival(): lax.all_to_all(blocks, axis, split_axis=0, concat_axis=0, tiled=True)  39.7 us
    all_to_all x1, waiting for transfers between devices, per_device(): lax.all_to_all(shared_rows, 'sp', split_axis=1, concat_axis=0, tiled=True)  23 us
    all_to_all x1, waiting for transfers between devices, summed_on_arrival(): lax.all_to_all(blocks, axis, split_axis=0, concat_axis=0, tiled=True)  12.2 us
    all_to_all x1, starting transfers between devices, per_device(): lax.all_to_all(shared_rows, 'sp', split_axis=1, concat_axis=0, tiled=True)  12 us
    all_to_all x1, waiting for transfers between devices, copy_for_each(): return lax.all_to_all(copies, axis, split_axis=0, concat_axis=0, tiled=True)  9.72 us
  transfers between devices with their start and end apart: 6, of which 5 were waited for; matrix products, arithmetic and copies ran while one was open for 4% of the time, Pallas kernels for 0%

commit v1 on v0

v1 whole, which is shorter than its diff:
```python
import functools

import jax
import jax.numpy as jnp
from jax import lax
from jax.experimental import pallas as pl
from jax.experimental.pallas import tpu as pltpu
from jax.sharding import PartitionSpec as P

PLANES, PLANE, TP, CAP = 8, 8, 4, 12
SP = PLANES * PLANE
ROWS = 2 * CAP
VMEM = pl.BlockSpec(memory_space=pltpu.VMEM)
BF, F32 = jnp.bfloat16, jnp.float32


def dot(a, b, dims=((1,), (0,))):
    return lax.dot_general(a, b, (dims, ((), ())), preferred_element_type=F32)


def device(sp, tp):
    return {"sp": sp, "tp": tp}


def plane_step(g):
    return ((g + 1) // 2) * (2 * (g % 2) - 1)


def greet_all(me, y, right, left):
    barrier = pltpu.get_barrier_semaphore()

    def signal(i, c):
        pl.semaphore_signal(barrier, inc=1, device_id=device((me + i) % SP, y))
        return c

    lax.fori_loop(1, SP, signal, 0)
    pl.semaphore_signal(barrier, inc=1, device_id=device(me, right))
    pl.semaphore_signal(barrier, inc=1, device_id=device(me, left))
    return barrier


def wait_bytes(ref, sem):
    pltpu.make_async_copy(ref, ref, sem).wait()


def pack_kernel(routes, weights, hidden, cot, send, own, select):
    me, y = lax.axis_index("sp"), lax.axis_index("tp")
    tokens, width = hidden.shape
    share = width // TP
    down = lax.broadcasted_iota(jnp.int32, (tokens, tokens), 0)
    across = lax.broadcasted_iota(jnp.int32, (tokens, tokens), 1)

    def as_row(column):
        return jnp.sum(
            jnp.where(down == across, column, jnp.zeros_like(column)), axis=0, keepdims=True
        )

    def count(match):
        return jnp.sum(jnp.where(match, 1.0, 0.0), axis=0, keepdims=True).astype(jnp.int32)

    c0, c1 = routes[:, 0:1], routes[:, 1:2]
    r0, r1 = as_row(c0), as_row(c1)
    w0, w1 = as_row(weights[:, 0:1]), as_row(weights[:, 1:2])
    earlier = down < across
    t0 = r0 * ROWS + count(earlier & (c0 == r0))
    t1 = r1 * ROWS + count(c0 == r1) + count(earlier & (c1 == r1))
    part = PLANE * ROWS
    row = lax.broadcasted_iota(jnp.int32, (part, tokens), 0)
    is_token_row = lax.broadcasted_iota(jnp.int32, (part, 1), 0) % ROWS < CAP

    def picks(g):
        slot = row + g * part
        h = jnp.where((t0 == slot) | (t1 == slot), 1.0, 0.0)
        s0, s1 = t0 + CAP == slot, t1 + CAP == slot
        s = jnp.where(s0 | s1, 1.0, 0.0)
        scale = jnp.sum(jnp.where(s0, w0, 0.0) + jnp.where(s1, w1, 0.0), axis=1, keepdims=True)
        return h.astype(BF), s.astype(BF), (h + s).astype(BF), jnp.where(is_token_row, 1.0, scale)

    mine = pl.ds(pl.multiple_of(y * share, share), share)

    def one(g, c):
        h, s, both, scale = picks(g)
        rows = (dot(h, hidden[:, mine]) + dot(s, cot[:, mine])) * scale
        send[pl.ds(g * PLANE, PLANE)] = rows.astype(BF).reshape(PLANE, ROWS, share)
        select[pl.ds(pl.multiple_of(g * part, part), part), :] = both
        return c

    lax.fori_loop(0, PLANES, one, 0)
    h, s, _, scale = picks(me // PLANE)
    for k in range(TP):
        cols = pl.ds(k * share, share)
        rows = (dot(h, hidden[:, cols]) + dot(s, cot[:, cols])) * scale
        own[k] = rows.astype(BF).reshape(PLANE, ROWS, share)


def pack(routes, weights, hidden, cot):
    tokens, width = hidden.shape
    share = width // TP
    return pl.pallas_call(
        pack_kernel,
        out_shape=(
            jax.ShapeDtypeStruct((SP, ROWS, share), BF),
            jax.ShapeDtypeStruct((TP, PLANE, ROWS, share), BF),
            jax.ShapeDtypeStruct((SP * ROWS, tokens), BF),
        ),
        in_specs=[VMEM] * 4,
        out_specs=(VMEM,) * 3,
        compiler_params=pltpu.CompilerParams(vmem_limit_bytes=40 * 2**20),
        name="pack",
    )(routes, weights, hidden, cot)


def dispatch_kernel(send, own, got, z_in, z_out, f_in, f_out, y_in, y_out):
    me, y = lax.axis_index("sp"), lax.axis_index("tp")
    z, cell = me // PLANE, me % PLANE
    right, left, far = (y + 1) % TP, (y + 3) % TP, (y + 2) % TP
    barrier = greet_all(me, y, right, left)
    got[y, me] = send[me]
    for k in range(1, TP):
        got[(y + k) % TP, me] = own[(y + k) % TP, cell]
    pl.semaphore_wait(barrier, SP + 1)

    def send_block(i, c):
        g, j = i // PLANE, i % PLANE
        to = ((z + plane_step(g) + PLANES) % PLANES) * PLANE + (cell + j) % PLANE
        pltpu.make_async_remote_copy(
            send.at[to], got.at[y, me], z_out, z_in.at[g], device_id=device(to, y)
        ).start()
        return c

    lax.fori_loop(1, SP, send_block, 0)
    near = (TP - 1) * (PLANE - 1)

    def send_full(i, c):
        j, s = (cell + 1 + i % (PLANE - 1)) % PLANE, (y + 1 + i // (PLANE - 1)) % TP
        pltpu.make_async_remote_copy(
            own.at[s, j], got.at[s, me], f_out, f_in, device_id=device(z * PLANE + j, y)
        ).start()
        return c

    lax.fori_loop(0, near, send_full, 0)

    def block(s, g, at=0, size=PLANE):
        source = (z - plane_step(g) + PLANES) % PLANES
        return got.at[s, pl.ds(source * PLANE + at, size)]

    def pass_on(s, g, k, to):
        ref = block(s, g) if k < 2 else block(s, g, (k - 2) * (PLANE // 2), PLANE // 2)
        return pltpu.make_async_remote_copy(
            ref, ref, y_out.at[k], y_in.at[k, g], device_id=device(me, to)
        )

    def step(g, c):
        @pl.when(g < PLANES)
        def _():
            wait_bytes(block(y, g), z_in.at[g])
            pass_on(y, g, 0, right).start()
            pass_on(y, g, 1, left).start()

        @pl.when(g > 1)
        def _():
            pass_on(left, g - 1, 0, left).wait_recv()
            pass_on(left, g - 1, 2, right).start()
            pass_on(right, g - 1, 1, right).wait_recv()
            pass_on(right, g - 1, 3, left).start()

        return c

    lax.fori_loop(1, PLANES + 1, step, 0)

    def last(g, c):
        pass_on(far, g, 2, right).wait_recv()
        pass_on(far, g, 3, left).wait_recv()
        return c

    lax.fori_loop(1, PLANES, last, 0)
    for k in range(4):
        size = PLANE if k < 2 else PLANE // 2
        wait_bytes(got.at[0, pl.ds(0, size * (PLANES - 1))], y_out.at[k])
    wait_bytes(got.at[0, pl.ds(0, PLANE - 1)], z_in.at[0])
    wait_bytes(got.at[0, pl.ds(0, near)], f_in)
    wait_bytes(got.at[0, pl.ds(0, near)], f_out)
    wait_bytes(got.at[0, pl.ds(0, SP - 1)], z_out)


def dispatch(send, own):
    dma = pltpu.SemaphoreType.DMA
    return pl.pallas_call(
        dispatch_kernel,
        out_shape=jax.ShapeDtypeStruct((TP, *send.shape), BF),
        in_specs=[VMEM] * 2,
        out_specs=VMEM,
        scratch_shapes=[dma((PLANES,)), dma(()), dma(()), dma(()), dma((4, PLANES)), dma((4,))],
        compiler_params=pltpu.CompilerParams(
            collective_id=0, has_side_effects=True, vmem_limit_bytes=40 * 2**20
        ),
        name="dispatch",
    )(send, own)


def expert_kernel(got, w_gate, w_up, w_down, part, d_pre_out, d_up_out, hid_out):
    share, hidden = got.shape[3], w_gate.shape[1]
    rows = PLANE * ROWS
    is_token = lax.broadcasted_iota(jnp.int32, (rows, 1), 0) % ROWS < CAP

    def one(g, c):
        blocks = pl.ds(g * PLANE, PLANE)
        pre_gate = pre_up = d_hid = jnp.zeros((rows, hidden), F32)
        for k in range(TP):
            x = got[k, blocks].reshape(rows, share)
            cols = pl.ds(k * share, share)
            pre_gate += dot(x, w_gate[cols, :])
            pre_up += dot(x, w_up[cols, :])
            d_hid += dot(x, w_down[:, cols], ((1,), (1,)))
        d_hid = pltpu.roll(d_hid, rows - CAP, 0)
        sigma = 1.0 / (1.0 + jnp.exp(-pre_gate))
        silu = pre_gate * sigma
        hid = silu * pre_up
        d_up = d_hid * silu
        d_pre = d_hid * pre_up * sigma * (1.0 + pre_gate * (1.0 - sigma))
        at = pl.ds(pl.multiple_of(g * rows, rows), rows)
        d_pre_out[at, :] = jnp.where(is_token, d_pre, 0.0).astype(BF)
        d_up_out[at, :] = jnp.where(is_token, d_up, 0.0).astype(BF)
        hid_out[at, :] = jnp.where(is_token, 0.0, pltpu.roll(hid, CAP, 0)).astype(BF)
        twice_pre = jnp.where(is_token, d_pre, pltpu.roll(d_pre, CAP, 0)).astype(BF)
        twice_up = jnp.where(is_token, d_up, pltpu.roll(d_up, CAP, 0)).astype(BF)
        for k in range(TP):
            cols = pl.ds(k * share, share)
            grad = dot(twice_pre, w_gate[cols, :], ((1,), (1,)))
            grad += dot(twice_up, w_up[cols, :], ((1,), (1,)))
            half = share // 2
            folded = jnp.where(is_token, grad[:, :half], grad[:, half:])
            part[k, blocks] = folded.astype(BF).reshape(PLANE, ROWS, half)
        return c

    lax.fori_loop(0, PLANES, one, 0)


def experts(got, w_gate, w_up, w_down):
    share, hidden = got.shape[3], w_gate.shape[1]
    flat = jax.ShapeDtypeStruct((SP * ROWS, hidden), BF)
    return pl.pallas_call(
        expert_kernel,
        out_shape=(jax.ShapeDtypeStruct((TP, SP, ROWS, share // 2), BF), flat, flat, flat),
        in_specs=[VMEM] * 4,
        out_specs=(VMEM,) * 4,
        compiler_params=pltpu.CompilerParams(vmem_limit_bytes=50 * 2**20),
        name="experts",
    )(got, w_gate, w_up, w_down)


def return_kernel(part, back, near_in, total_in, sums, a_in, a_out, b_in, b_out, z_in, z_out):
    me, y = lax.axis_index("sp"), lax.axis_index("tp")
    z, cell = me // PLANE, me % PLANE
    right, left, far = (y + 1) % TP, (y + 3) % TP, (y + 2) % TP
    half = PLANE // 2
    pl.semaphore_wait(greet_all(me, y, right, left), SP + 1)

    def source(i):
        return (z + plane_step(PLANES - 1 - i) + PLANES) % PLANES

    def far_half(i, k, to):
        at = source(i) * PLANE + k * half
        return pltpu.make_async_remote_copy(
            part.at[far, pl.ds(at, half)],
            near_in.at[k, i],
            a_out.at[k],
            a_in.at[k, i],
            device_id=device(me, to),
        )

    def near_sum(i, k, to):
        return pltpu.make_async_remote_copy(
            part.at[to, pl.ds(source(i) * PLANE, PLANE)],
            total_in.at[k, i],
            b_out.at[k],
            b_in.at[k, i],
            device_id=device(me, to),
        )

    def start(i, c):
        far_half(i, 0, right).start()
        far_half(i, 1, left).start()
        return c

    def add(i, k, to):
        at = pl.ds(source(i) * PLANE + k * half, half)
        part[to, at] = (part[to, at].astype(F32) + near_in[k, i].astype(F32)).astype(BF)

    def send_back(i, j):
        to = source(i) * PLANE + (cell + j) % PLANE
        pltpu.make_async_remote_copy(
            sums.at[to], back.at[me], z_out, z_in, device_id=device(to, y)
        ).start()

    lax.fori_loop(0, 2, start, 0)

    def step(i, c):
        @pl.when(i < PLANES)
        def _():
            far_half(i, 0, right).wait_recv()
            add(i, 0, right)
            far_half(i, 1, left).wait_recv()
            add(i, 1, left)

            @pl.when(i + 2 < PLANES)
            def _():
                start(i + 2, 0)

            near_sum(i, 0, right).start()
            near_sum(i, 1, left).start()

        @pl.when(i > 0)
        def _():
            p = i - 1
            near_sum(p, 0, right).wait_recv()
            near_sum(p, 1, left).wait_recv()
            at = pl.ds(source(p) * PLANE, PLANE)
            sums[at] = (
                part[y, at].astype(F32) + total_in[0, p].astype(F32) + total_in[1, p].astype(F32)
            ).astype(BF)

            @pl.when(p < PLANES - 1)
            def _():
                send_back(p, 0)

            lax.fori_loop(1, PLANE, lambda j, d: (send_back(p, j), d)[1], 0)

        return c

    lax.fori_loop(0, PLANES + 1, step, 0)
    back[me] = sums[me]
    for k in range(2):
        wait_bytes(part.at[0, pl.ds(0, SP // 2)], a_out.at[k])
        wait_bytes(part.at[0], b_out.at[k])
    wait_bytes(part.at[0, pl.ds(0, SP - 1)], z_in)
    wait_bytes(part.at[0, pl.ds(0, SP - 1)], z_out)


def return_rows(part):
    dma = pltpu.SemaphoreType.DMA
    rows, half = part.shape[2:]
    return pl.pallas_call(
        return_kernel,
        out_shape=jax.ShapeDtypeStruct((SP, rows, half), BF),
        in_specs=[VMEM],
        out_specs=VMEM,
        scratch_shapes=[
            pltpu.VMEM((2, PLANES, PLANE // 2, rows, half), BF),
            pltpu.VMEM((2, PLANES, PLANE, rows, half), BF),
            pltpu.VMEM((SP, rows, half), BF),
            dma((2, PLANES)),
            dma((2,)),
            dma((2, PLANES)),
            dma((2,)),
            dma(()),
            dma(()),
        ],
        input_output_aliases={},
        compiler_params=pltpu.CompilerParams(
            collective_id=1, has_side_effects=True, vmem_limit_bytes=40 * 2**20
        ),
        name="return_rows",
    )(part)


def combine_kernel(select, back, cot, full, y_in, y_out):
    me, y = lax.axis_index("sp"), lax.axis_index("tp")
    right, left, far = (y + 1) % TP, (y + 3) % TP, (y + 2) % TP
    tokens, share = full.shape[1:]
    half = share // 2
    barrier = pltpu.get_barrier_semaphore()
    pl.semaphore_signal(barrier, inc=1, device_id=device(me, right))
    pl.semaphore_signal(barrier, inc=1, device_id=device(me, left))
    slots = SP * ROWS
    is_token = lax.broadcasted_iota(jnp.int32, (slots, 1), 0) % ROWS < CAP
    rows = back[...].reshape(slots, half)
    zero = jnp.zeros_like(rows)
    for k, kept in enumerate((jnp.where(is_token, rows, zero), jnp.where(is_token, zero, rows))):
        cols = pl.ds(pl.multiple_of(y * share + k * half, half), half)
        total = cot[:, cols].astype(F32) + dot(select[...], kept, ((0,), (0,)))
        full[y, :, pl.ds(k * half, half)] = total.astype(BF)
    pl.semaphore_wait(barrier, 2)

    def pass_on(s, k, to):
        ref = full.at[s] if k < 2 else full.at[s, pl.ds((k - 2) * (tokens // 2), tokens // 2)]
        return pltpu.make_async_remote_copy(
            ref, ref, y_out.at[k], y_in.at[k], device_id=device(me, to)
        )

    sends = [pass_on(y, 0, right), pass_on(y, 1, left)]
    for copy in sends:
        copy.start()
    pass_on(left, 0, left).wait_recv()
    sends.append(pass_on(left, 2, right))
    sends[-1].start()
    pass_on(right, 1, right).wait_recv()
    sends.append(pass_on(right, 3, left))
    sends[-1].start()
    pass_on(far, 2, right).wait_recv()
    pass_on(far, 3, left).wait_recv()
    for copy in sends:
        copy.wait_send()


def combine(select, back, cot):
    tokens, width = cot.shape
    dma = pltpu.SemaphoreType.DMA
    return pl.pallas_call(
        combine_kernel,
        out_shape=jax.ShapeDtypeStruct((TP, tokens, width // TP), BF),
        in_specs=[VMEM] * 3,
        out_specs=VMEM,
        scratch_shapes=[dma((4,)), dma((4,))],
        compiler_params=pltpu.CompilerParams(
            collective_id=2, has_side_effects=True, vmem_limit_bytes=40 * 2**20
        ),
        name="combine",
    )(select, back, cot)


def from_behind(x, axis, by):
    devices = lax.axis_size(axis)
    pairs = [(i, i + by) for i in range(devices) if 0 <= i + by < devices]
    return lax.ppermute(x, axis, pairs)


def per_device(
    hidden_in, cotangent, routes, routing_weights, w_gate, w_up, w_down, b_gate, c_gate, x_in, taps, w_out
):
    tokens, width = hidden_in.shape
    share = width // TP
    y = lax.axis_index("tp")
    send, own, select = pack(routes, routing_weights, hidden_in, cotangent)
    got = dispatch(send, own)
    part, d_pre, d_up, hid = experts(got, w_gate[0], w_up[0], w_down[0])
    rows = got.reshape(TP, SP * ROWS, share)
    back = return_rows(part)
    full = combine(select, back, cotangent)
    residual_grad = lax.dynamic_index_in_dim(full, y, 0, keepdims=False)

    def weight_grad(d):
        grad = jnp.einsum("krd,rf->kdf", rows, d, preferred_element_type=F32)
        return grad.astype(BF).reshape(1, width, -1)

    grad_gate, grad_up = weight_grad(d_pre), weight_grad(d_up)
    grad_down = jnp.einsum("rf,krd->fkd", hid, rows, preferred_element_type=F32)
    grad_down = grad_down.astype(BF).reshape(1, -1, width)

    taps_f = taps.astype(F32)
    gated = c_gate.astype(F32) * x_in.astype(F32)
    padded = jnp.concatenate([from_behind(gated[tokens - 2 :], "sp", 1), gated], axis=0)
    conv = (
        taps_f[0] * padded[0:tokens]
        + taps_f[1] * padded[1 : tokens + 1]
        + taps_f[2] * padded[2 : tokens + 2]
    )
    b_f = b_gate.astype(F32)
    y_short = (b_f * conv).astype(BF)
    w_parts = w_out.reshape(TP, share, -1)
    d_y = jnp.einsum("ktd,kdc->tc", full, w_parts, preferred_element_type=F32)
    grad_b = (d_y * conv).astype(BF)
    d_conv = b_f * d_y
    later = jnp.concatenate([d_conv, from_behind(d_conv[0:2], "sp", -1)], axis=0)
    d_v = (
        taps_f[2] * later[0:tokens]
        + taps_f[1] * later[1 : tokens + 1]
        + taps_f[0] * later[2 : tokens + 2]
    )
    grad_c = (d_v * x_in.astype(F32)).astype(BF)
    grad_x = (d_v * c_gate.astype(F32)).astype(BF)
    out_part = jnp.einsum("ktd,tc->kdc", full, y_short, preferred_element_type=F32).astype(BF)
    out_part = out_part.reshape(SP, width // SP, -1)
    arrived = lax.all_to_all(out_part, "sp", split_axis=0, concat_axis=0, tiled=True)
    out_proj_grad = arrived.astype(F32).sum(axis=0)
    return (grad_gate, grad_up, grad_down, out_proj_grad, residual_grad, grad_b, grad_c, grad_x)


def solution(mesh):
    seq, both = P("sp", None), P("sp", "tp")
    return jax.shard_map(
        per_device,
        mesh=mesh,
        in_specs=(
            seq,
            seq,
            seq,
            seq,
            P("sp", None, "tp"),
            P("sp", None, "tp"),
            P("sp", "tp", None),
            both,
            both,
            both,
            P(None, "tp"),
            P(None, "tp"),
        ),
        out_specs=(
            P("sp", None, "tp"),
            P("sp", None, "tp"),
            P("sp", "tp", None),
            both,
            both,
            both,
            both,
            both,
        ),
        check_vma=False,
    )
```

time: 340 us -> 203 us (0.60)
  Pallas kernels: 0 us -> 144 us
  waiting for transfers between devices: 112 us -> 2.99 us
  blocking collectives: 102 us -> 0 us
  local copies, waits for them, and re-layouts: 40.7 us -> 15.6 us
  between operations: 14.6 us -> 0.84 us
  starting transfers between devices: 28.6 us -> 15.5 us
  other arithmetic: 15.7 us -> 5.74 us
  matrix products: 25.4 us -> 17.4 us
    pallas_call x0 -> x5, Pallas kernels: none -> 144 us  [the longest x1 67 us: dispatch(): pl.pallas_call(dispatch_kernel, out_shape=jax.ShapeDtypeStruct((TP, *send...]
    all_to_all x2 -> x0, blocking collectives: 102 us -> none  [the longest x1 62.5 us: in_one_piece(): lax.all_to_all(both, axis, split_axis=split_dim, concat_axis=concat_dim,...]
    all_gather x1 -> x0, waiting for transfers between devices: 66 us -> none  [sent_together(): lax.all_gather(both, axis, axis=dim, tiled=True)]
    all_to_all x3 -> x1, waiting for transfers between devices: 44.9 us -> 2.99 us  [per_device(): lax.all_to_all(out_part, 'sp', split_axis=0, concat_axis=0, tiled=True)]
    gather x5 -> x0, local copies, waits for them, and re-layouts: 15.7 us -> none  [the longest x2 5.42 us: per_device(): rows_src[token_of]]
    all_to_all x3 -> x1, starting transfers between devices: 22.3 us -> 8.56 us  [per_device(): lax.all_to_all(out_part, 'sp', split_axis=0, concat_axis=0, tiled=True)]
    dot_general x10 -> x5, matrix products: 25.4 us -> 17.4 us  [the longest x2 8.73 us: weight_grad(): grad = jnp.einsum('krd,rf->kdf', rows, d, preferred_element_type=F32)]
    reshape x3 -> x0, local copies, waits for them, and re-layouts: 5.55 us -> none  [the longest x2 5.41 us: cut_along(): return jnp.moveaxis(x.reshape(*before, devices, -1, *after), dim, 0)]
  transfers between devices with their start and end apart: 6 -> 3, of which waited for: 5 -> 1; matrix products, arithmetic and copies ran while one was open for 4% -> 12% of each run, Pallas kernels for 0% -> 71%
where the time goes in v1:
time: 203 us; the launch traced here: 202 us
  Pallas kernels  144 us (71%)
  matrix products  17.4 us (9%)
  local copies, waits for them, and re-layouts  15.6 us (8%)
  starting transfers between devices  15.5 us (8%)
  other arithmetic  5.74 us (3%)
  waiting for transfers between devices  2.99 us (1%)
    pallas_call x1, Pallas kernels, dispatch(): pl.pallas_call(dispatch_kernel, out_shape=jax.ShapeDtypeStruct((TP, *send...  67 us
    pallas_call x1, Pallas kernels, return_rows(): pl.pallas_call(return_kernel, out_shape=jax.ShapeDtypeStruct((SP, rows, h...  39.2 us
    pallas_call x1, Pallas kernels, experts(): pl.pallas_call(expert_kernel, out_shape=(jax.ShapeDtypeStruct((TP, SP, RO...  22.7 us
    pallas_call x1, Pallas kernels, combine(): pl.pallas_call(combine_kernel, out_shape=jax.ShapeDtypeStruct((TP, tokens...  11.5 us
    unnamed x37, local copies, waits for them, and re-layouts  10.9 us
    dot_general x2, matrix products, weight_grad(): grad = jnp.einsum('krd,rf->kdf', rows, d, preferred_element_type=F32)  8.73 us
    all_to_all x1, starting transfers between devices, per_device(): lax.all_to_all(out_part, 'sp', split_axis=0, concat_axis=0, tiled=True)  8.56 us
    ppermute x2, starting transfers between devices, from_behind(): return lax.ppermute(x, axis, pairs)  6.93 us
  transfers between devices with their start and end apart: 3, of which 1 were waited for; matrix products, arithmetic and copies ran while one was open for 12% of the time, Pallas kernels for 71%

profile of v1, /device:TPU:1, one launch (start us, length us, event | category | flops | bytes accessed | tf_op | source)
XLA Modules:
  0.0 202.3 jit_solution(7239699182929055873)
XLA Ops:
  0.6 1.1 convert_multiply_fusion.1
  1.7 4.5 %collective-permute-start = (f32[2,256]{1,0:T(2,128)S(1)}, f32[2,256]{1,0:T(2,128)S(1)}, u32[]{:S(2)}, u32[]{:S(2)}) collective-permute-start(f32[2,256]{1,0:T(2,128)S(1)} %slice.40), channel_id=1, source_target_pairs={{0,4},{4,8},{8,12},{12,16},{16,20},{20,24},{24,28},{28,32},{32,36}... | collective-permute-start | bytes 6152 | tf_op jit(solution)/shard_map/ppermute | solution.py:425
  8.7 1.2 copy-done.3
  9.9 1.2 copy-done.7
  11.1 3.7 %pack.1 = (bf16[64,24,512]{2,1,0:T(8,128)(2,1)S(1)}, bf16[4,8,24,512]{3,2,1,0:T(8,128)(2,1)S(1)}, bf16[1536,256]{1,0:T(8,128)(2,1)S(1)}) custom-call(s32[256,2]{1,0:T(8,128)S(1)} %copy.26.routes, f32[256,2]{1,0:T(8,128)S(1)} %copy.27.weights, bf16[256,2048]{1,0:T(8,128)(2,1)S(1)} %copy-done.7, bf16[256,2048]{1,0:T(8,128)(2,1)S(1)} %copy-done.3), custom_call_target="tpu_custom_call" | custom-call | tf_op jit(solution)/shard_map/pack/pallas_call | solution.py:99
  14.9 67.0 %dispatch.1.got = bf16[4,64,24,512]{3,2,1,0:T(8,128)(2,1)S(1)} custom-call(bf16[64,24,512]{2,1,0:T(8,128)(2,1)S(1)} %get-tuple-element.15.send, bf16[4,8,24,512]{3,2,1,0:T(8,128)(2,1)S(1)} %get-tuple-element.16.own), custom_call_target="tpu_custom_call" | custom-call | tf_op jit(solution)/shard_map/dispatch/pallas_call | solution.py:188
  81.9 2.6 %copy-done.1 = bf16[4,64,24,512]{3,2,1,0:T(8,128)(2,1)} copy-done((bf16[4,64,24,512]{3,2,1,0:T(8,128)(2,1)}, bf16[4,64,24,512]{3,2,1,0:T(8,128)(2,1)S(1)}, u32[]{:S(2)}) %copy-start.1) | copy-done | bytes 6291480
  84.6 22.7 %experts.1 = (bf16[4,64,24,256]{3,2,1,0:T(8,128)(2,1)}, bf16[1536,256]{1,0:T(8,128)(2,1)S(1)}, bf16[1536,256]{1,0:T(8,128)(2,1)S(1)}, bf16[1536,256]{1,0:T(8,128)(2,1)S(1)}) custom-call(bf16[4,64,24,512]{3,2,1,0:T(8,128)(2,1)} %copy-done.1, bf16[2048,256]{1,0:T(8,128)(2,1)S(1)} %bitcast.40, bf16[2048,256]{1,0:T(8,128)(2,1)} %bitcast.42, ...), custom_call_target="tpu_custom_call" | custom-call | tf_op jit(solution)/shard_map/experts/pallas_call | solution.py:242
  107.3 2.7 %copy-done.5 = bf16[4,64,24,256]{3,2,1,0:T(8,128)(2,1)S(1)} copy-done((bf16[4,64,24,256]{3,2,1,0:T(8,128)(2,1)S(1)}, bf16[4,64,24,256]{3,2,1,0:T(8,128)(2,1)}, u32[]{:S(2)}) %copy-start.5) | copy-done | bytes 3145752
  110.0 39.2 %return_rows.1.back = bf16[64,24,256]{2,1,0:T(8,128)(2,1)S(1)} custom-call(bf16[4,64,24,256]{3,2,1,0:T(8,128)(2,1)S(1)} %copy-done.5), custom_call_target="tpu_custom_call" | custom-call | tf_op jit(solution)/shard_map/return_rows/pallas_call | solution.py:343
  149.3 11.5 %combine.1 = bf16[4,256,512]{2,1,0:T(8,128)(2,1)S(1)} custom-call(bf16[1536,256]{1,0:T(8,128)(2,1)S(1)} %get-tuple-element.20.select, bf16[64,24,256]{2,1,0:T(8,128)(2,1)S(1)} %return_rows.1.back, bf16[256,2048]{1,0:T(8,128)(2,1)S(1)} %copy-done.4), custom_call_target="tpu_custom_call" | custom-call | tf_op jit(solution)/shard_map/combine/pallas_call | solution.py:409
  160.8 1.2 multiply_convert_fusion
  162.1 1.6 convolution_convert_fusion
  163.6 8.6 %all-to-all-start = ((bf16[64,32,256]{2,1,0:T(8,128)(2,1)}), bf16[64,32,256]{2,1,0:T(8,128)(2,1)}, u32[]{:S(2)}, u32[]{:S(2)}) async-start(bf16[64,32,256]{2,1,0:T(8,128)(2,1)} %bitcast.14), calls=%async_computation | async-start | bytes 2097152 | tf_op jit(solution)/shard_map/all_to_all | solution.py:474
  172.2 5.9 %convolution_convert_fusion.1 = bf16[256,4,512]{2,0,1:T(8,128)(2,1)} fusion(bf16[4,1536,512]{2,1,0:T(8,128)(2,1)} %bitcast.35, bf16[1536,256]{1,0:T(8,128)(2,1)} %copy-done.11), kind=kOutput, calls=%fused_computation.2 | convolution fusion | flops 1611137024 | bytes 8126464 | tf_op jit(solution)/shard_map/rf,krd->fkd/dot_general | solution.py:447
  178.2 5.9 %convolution_convert_fusion.2 = bf16[4,512,256]{2,1,0:T(8,128)(2,1)} fusion(bf16[4,1536,512]{2,1,0:T(8,128)(2,1)} %bitcast.36, bf16[1536,256]{1,0:T(8,128)(2,1)} %copy-done.10), kind=kOutput, calls=%fused_computation.3 | convolution fusion | flops 1611137024 | bytes 8126464 | tf_op jit(solution)/shard_map/krd,rf->kdf/dot_general | solution.py:443
  184.1 2.8 %convolution_convert_fusion.3 = bf16[4,512,256]{2,1,0:T(8,128)(2,1)} fusion(bf16[4,1536,512]{2,1,0:T(8,128)(2,1)S(1)} %bitcast.39, bf16[1536,256]{1,0:T(8,128)(2,1)S(1)} %copy-done.9), kind=kOutput, calls=%fused_computation.4 | convolution fusion | flops 1611137024 | bytes 8126464 | tf_op jit(solution)/shard_map/krd,rf->kdf/dot_general | solution.py:443
  187.6 2.4 %collective-permute-start.1 = (f32[2,256]{1,0:T(2,128)S(1)}, f32[2,256]{1,0:T(2,128)S(1)}, u32[]{:S(2)}, u32[]{:S(2)}) collective-permute-start(f32[2,256]{1,0:T(2,128)S(1)} %slice.45), channel_id=1, source_target_pairs={{4,0},{8,4},{12,8},{16,12},{20,16},{24,20},{28,24},{32,28},{36,32}... | collective-permute-start | bytes 6152 | tf_op jit(solution)/shard_map/ppermute | solution.py:425
  190.1 1.7 dynamic-slice_bitcast_fusion
  191.7 1.5 copy.31
  193.2 1.4 copy.33
  194.6 1.9 fusion.12
  197.3 3.0 %all-to-all-done = bf16[64,32,256]{2,1,0:T(8,128)(2,1)} async-done(((bf16[64,32,256]{2,1,0:T(8,128)(2,1)}), bf16[64,32,256]{2,1,0:T(8,128)(2,1)}, u32[]{:S(2)}, u32[]{:S(2)}) %all-to-all-start) | async-done | bytes 1048608 | tf_op jit(solution)/shard_map/all_to_all | solution.py:474
  200.3 2.0 convert_reduce_fusion
  (39 shorter events, 3.9 us)
Async XLA Ops:
  0.6 160.2 %copy-start = (bf16[2048,256]{1,0:T(8,128)(2,1)S(1)}, bf16[2048,256]{1,0:T(8,128)(2,1)}, u32[]{:S(2)}) copy-start(bf16[2048,256]{1,0:T(8,128)(2,1)} %param.23) | copy-start | bytes 3145732
  1.7 159.1 %collective-permute-start = (f32[2,256]{1,0:T(2,128)S(1)}, f32[2,256]{1,0:T(2,128)S(1)}, u32[]{:S(2)}, u32[]{:S(2)}) collective-permute-start(f32[2,256]{1,0:T(2,128)S(1)} %slice.40), channel_id=1, source_target_pairs={{0,4},{4,8},{8,12},{12,16},{16,20},{20,24},{24,28},{28,32},{32,36}... | collective-permute-start | bytes 6152 | tf_op jit(solution)/shard_map/ppermute | solution.py:425
  8.7 1.2 copy-start.3
  9.9 1.2 copy-start.7
  11.1 73.4 %copy-start.6 = (bf16[1,2048,256]{2,1,0:T(8,128)(2,1)S(1)}, bf16[1,2048,256]{2,1,0:T(8,128)(2,1)}, u32[]{:S(2)}) copy-start(bf16[1,2048,256]{2,1,0:T(8,128)(2,1)} %param.16) | copy-start | bytes 3145732
  81.9 2.7 %copy-start.1 = (bf16[4,64,24,512]{3,2,1,0:T(8,128)(2,1)}, bf16[4,64,24,512]{3,2,1,0:T(8,128)(2,1)S(1)}, u32[]{:S(2)}) copy-start(bf16[4,64,24,512]{3,2,1,0:T(8,128)(2,1)S(1)} %dispatch.1.got) | copy-start | bytes 18874372
  84.6 64.7 %copy-start.4 = (bf16[256,2048]{1,0:T(8,128)(2,1)S(1)}, bf16[256,2048]{1,0:T(8,128)(2,1)}, u32[]{:S(2)}) copy-start(bf16[256,2048]{1,0:T(8,128)(2,1)} %cot.3) | copy-start | bytes 3145732
  84.6 76.3 %copy-start.14 = (bf16[256,256]{1,0:T(8,128)(2,1)S(1)}, bf16[256,256]{1,0:T(8,128)(2,1)}, u32[]{:S(2)}) copy-start(bf16[256,256]{1,0:T(8,128)(2,1)} %param.19) | copy-start | bytes 393220
  107.3 56.3 %copy-start.8 = (bf16[1536,256]{1,0:T(8,128)(2,1)}, bf16[1536,256]{1,0:T(8,128)(2,1)S(1)}, u32[]{:S(2)}) copy-start(bf16[1536,256]{1,0:T(8,128)(2,1)S(1)} %get-tuple-element.17) | copy-start | bytes 2359300
  107.3 56.3 %copy-start.10 = (bf16[1536,256]{1,0:T(8,128)(2,1)}, bf16[1536,256]{1,0:T(8,128)(2,1)S(1)}, u32[]{:S(2)}) copy-start(bf16[1536,256]{1,0:T(8,128)(2,1)S(1)} %get-tuple-element.18) | copy-start | bytes 2359300
  107.3 56.3 %copy-start.11 = (bf16[1536,256]{1,0:T(8,128)(2,1)}, bf16[1536,256]{1,0:T(8,128)(2,1)S(1)}, u32[]{:S(2)}) copy-start(bf16[1536,256]{1,0:T(8,128)(2,1)S(1)} %get-tuple-element.19) | copy-start | bytes 2359300
  107.3 2.7 %copy-start.5 = (bf16[4,64,24,256]{3,2,1,0:T(8,128)(2,1)S(1)}, bf16[4,64,24,256]{3,2,1,0:T(8,128)(2,1)}, u32[]{:S(2)}) copy-start(bf16[4,64,24,256]{3,2,1,0:T(8,128)(2,1)} %get-tuple-element.21.part) | copy-start | bytes 9437188
  160.8 1.3 copy-start.2
  163.6 36.7 %all-to-all-start = ((bf16[64,32,256]{2,1,0:T(8,128)(2,1)}), bf16[64,32,256]{2,1,0:T(8,128)(2,1)}, u32[]{:S(2)}, u32[]{:S(2)}) async-start(bf16[64,32,256]{2,1,0:T(8,128)(2,1)} %bitcast.14), calls=%async_computation | async-start | bytes 2097152 | tf_op jit(solution)/shard_map/all_to_all | solution.py:474
  172.2 11.9 %slice-start = ((s8[6291456]{0:T(1024)(128)(4,1)}), s8[2097152]{0:T(1024)(128)(4,1)S(1)}, s32[]{:S(2)}) async-start(s8[6291456]{0:T(1024)(128)(4,1)} %bitcast.37), calls=%async_computation.1 | async-start | bytes 4194304
  178.2 5.9 %slice-start.1 = ((s8[6291456]{0:T(1024)(128)(4,1)}), s8[4194304]{0:T(1024)(128)(4,1)S(1)}, s32[]{:S(2)}) async-start(s8[6291456]{0:T(1024)(128)(4,1)} %bitcast.37), calls=%async_computation.2 | async-start | bytes 8388608
  178.2 5.9 %copy-start.9 = (bf16[1536,256]{1,0:T(8,128)(2,1)S(1)}, bf16[1536,256]{1,0:T(8,128)(2,1)}, u32[]{:S(2)}) copy-start(bf16[1536,256]{1,0:T(8,128)(2,1)} %copy-done.8) | copy-start | bytes 2359300
  184.1 10.6 %copy-start.12 = (bf16[256,256]{1,0:T(8,128)(2,1)S(1)}, bf16[256,256]{1,0:T(8,128)(2,1)}, u32[]{:S(2)}) copy-start(bf16[256,256]{1,0:T(8,128)(2,1)} %param.20) | copy-start | bytes 393220
  184.1 12.5 %copy-start.13 = (bf16[256,256]{1,0:T(8,128)(2,1)S(1)}, bf16[256,256]{1,0:T(8,128)(2,1)}, u32[]{:S(2)}) copy-start(bf16[256,256]{1,0:T(8,128)(2,1)} %param.21) | copy-start | bytes 393220
  187.6 7.0 %collective-permute-start.1 = (f32[2,256]{1,0:T(2,128)S(1)}, f32[2,256]{1,0:T(2,128)S(1)}, u32[]{:S(2)}, u32[]{:S(2)}) collective-permute-start(f32[2,256]{1,0:T(2,128)S(1)} %slice.45), channel_id=1, source_target_pairs={{4,0},{8,4},{12,8},{16,12},{20,16},{24,20},{28,24},{32,28},{36,32}... | collective-permute-start | bytes 6152 | tf_op jit(solution)/shard_map/ppermute | solution.py:425

commit v2 on v0

v2 whole, which is shorter than its diff:
```python
import functools

import jax
import jax.numpy as jnp
from jax import lax
from jax.experimental import pallas as pl
from jax.experimental.pallas import tpu as pltpu
from jax.sharding import PartitionSpec as P

PLANES, PLANE, TP, CAP = 8, 8, 4, 12
SP = PLANES * PLANE
ROWS = 2 * CAP
VMEM = pl.BlockSpec(memory_space=pltpu.VMEM)
BF, F32 = jnp.bfloat16, jnp.float32


def dot(a, b, dims=((1,), (0,))):
    return lax.dot_general(a, b, (dims, ((), ())), preferred_element_type=F32)


def device(sp, tp):
    return {"sp": sp, "tp": tp}


def plane_step(g):
    return ((g + 1) // 2) * (2 * (g % 2) - 1)


def greet_all(me, y, right, left):
    barrier = pltpu.get_barrier_semaphore()

    def signal(i, c):
        pl.semaphore_signal(barrier, inc=1, device_id=device((me + i) % SP, y))
        return c

    lax.fori_loop(1, SP, signal, 0)
    pl.semaphore_signal(barrier, inc=1, device_id=device(me, right))
    pl.semaphore_signal(barrier, inc=1, device_id=device(me, left))
    return barrier


def wait_bytes(ref, sem):
    pltpu.make_async_copy(ref, ref, sem).wait()


def kernel(
    routes, weights, taps, hidden_hbm, cot_hbm, w_gate_hbm, w_up_hbm, w_down_hbm, w_out_hbm, b_hbm, c_hbm, x_hbm,
    grad_gate, grad_up, grad_down, grad_out, residual, grad_b, grad_c, grad_x,
    hidden, cot, w_gate, w_up, w_down, w_out, b_gate, c_gate, x_in,
    send, own, select, got, part, near_in, total_in, sums, back, d_both, hid_rows, full, y_short,
    edge, edge_in, outs, outs_in, plane_sum, plane_in,
    ld, z_in, z_out, f_in, f_out, y_in, y_out, a_in, a_out, b_in, b_out, r_in, r_out,
    h_in, h_out, e_in, e_out, o_in, o_out, q_in, q_out,
):
    me, y = lax.axis_index("sp"), lax.axis_index("tp")
    z, cell = me // PLANE, me % PLANE
    right, left, far = (y + 1) % TP, (y + 3) % TP, (y + 2) % TP
    tokens, width = hidden.shape
    share = width // TP
    half_share = share // 2
    part_rows = PLANE * ROWS
    slots = SP * ROWS
    mid = PLANE // 2
    ff = w_gate.shape[1]

    loads = [
        pltpu.make_async_copy(a, b, ld.at[i])
        for i, (a, b) in enumerate(
            (
                (hidden_hbm, hidden),
                (cot_hbm, cot),
                (c_hbm, c_gate),
                (x_hbm, x_in),
                (w_gate_hbm, w_gate),
                (w_up_hbm, w_up),
                (w_down_hbm, w_down),
                (b_hbm, b_gate),
                (w_out_hbm, w_out),
            )
        )
    ]
    for load in loads:
        load.start()
    barrier = greet_all(me, y, right, left)

    down = lax.broadcasted_iota(jnp.int32, (tokens, tokens), 0)
    across = lax.broadcasted_iota(jnp.int32, (tokens, tokens), 1)

    def count(match):
        return jnp.sum(jnp.where(match, 1.0, 0.0), axis=0, keepdims=True).astype(jnp.int32)

    r0, r1 = routes[0:1, :], routes[1:2, :]
    w0, w1 = weights[0:1, :], weights[1:2, :]
    c0 = jnp.sum(jnp.where(down == across, r0, 0), axis=1, keepdims=True)
    c1 = jnp.sum(jnp.where(down == across, r1, 0), axis=1, keepdims=True)
    earlier = down < across
    t0 = r0 * ROWS + count(earlier & (c0 == r0))
    t1 = r1 * ROWS + count(c0 == r1) + count(earlier & (c1 == r1))
    row = lax.broadcasted_iota(jnp.int32, (part_rows, tokens), 0)
    is_token = lax.broadcasted_iota(jnp.int32, (part_rows, 1), 0) % ROWS < CAP

    def picks(plane):
        slot = row + plane * part_rows
        h = jnp.where((t0 == slot) | (t1 == slot), 1.0, 0.0)
        s0, s1 = t0 + CAP == slot, t1 + CAP == slot
        s = jnp.where(s0 | s1, 1.0, 0.0)
        scale = jnp.sum(jnp.where(s0, w0, 0.0) + jnp.where(s1, w1, 0.0), axis=1, keepdims=True)
        select[pl.ds(pl.multiple_of(plane * part_rows, part_rows), part_rows), :] = (h + s).astype(BF)
        return h.astype(BF), s.astype(BF), jnp.where(is_token, 1.0, scale)

    def plane_of(g, sign):
        return (z + sign * plane_step(g) + PLANES) % PLANES

    mine = pl.ds(pl.multiple_of(y * share, share), share)

    def pack(g):
        plane = plane_of(g, 1)
        h, s, scale = picks(plane)
        rows = (dot(h, hidden[:, mine]) + dot(s, cot[:, mine])) * scale
        send[pl.ds(plane * PLANE, PLANE)] = rows.astype(BF).reshape(PLANE, ROWS, share)

    def send_group(g):
        def one(j, c):
            to = plane_of(g, 1) * PLANE + (cell + j) % PLANE
            pltpu.make_async_remote_copy(
                send.at[to], got.at[y, me], z_out, z_in.at[g], device_id=device(to, y)
            ).start()
            return c

        lax.fori_loop(0, PLANE, one, 0)

    loads[0].wait()
    loads[1].wait()
    pack(1)
    pl.semaphore_wait(barrier, SP + 1)

    def pack_ahead(g, c):
        pack(g + 1)
        send_group(g)
        return c

    lax.fori_loop(1, 3, pack_ahead, 0)
    h, s, scale = picks(z)
    for k in range(TP):
        cols = pl.ds(k * share, share)
        rows = (dot(h, hidden[:, cols]) + dot(s, cot[:, cols])) * scale
        own[k] = rows.astype(BF).reshape(PLANE, ROWS, share)
    send_group(3)
    for k in range(TP):
        got[k, me] = own[k, cell]

    def send_full(i, c):
        j, k = (cell + 1 + i % (PLANE - 1)) % PLANE, i // (PLANE - 1)
        pltpu.make_async_remote_copy(
            own.at[k, j], got.at[k, me], f_out, f_in, device_id=device(z * PLANE + j, y)
        ).start()
        return c

    near = TP * (PLANE - 1)
    lax.fori_loop(0, near, send_full, 0)
    pack(4)
    lax.fori_loop(4, PLANES - 1, pack_ahead, 0)

    loads[2].wait()
    loads[3].wait()
    edge[0] = c_gate[tokens - 8 :, :].astype(F32) * x_in[tokens - 8 :, :].astype(F32)
    send_group(PLANES - 1)

    def edge_copy(k, by):
        return pltpu.make_async_remote_copy(
            edge.at[k], edge_in.at[k], h_out.at[k], h_in.at[k], device_id=device((me + by + SP) % SP, y)
        )

    edge_copy(0, 1).start()
    for load in loads[4:7]:
        load.wait()

    def block(k, g, at=0, size=PLANE):
        return got.at[k, pl.ds(plane_of(g, -1) * PLANE + at, size)]

    def pass_on(s, g, k, to):
        ref = block(s, g) if k < 2 else block(s, g, (k - 2) * mid, mid)
        return pltpu.make_async_remote_copy(
            ref, ref, y_out.at[k], y_in.at[k, g], device_id=device(me, to)
        )

    def expert_rows(g):
        plane = plane_of(g, -1)
        blocks = pl.ds(plane * PLANE, PLANE)
        pre_gate = pre_up = d_hid = jnp.zeros((part_rows, ff), F32)
        for k in range(TP):
            x = got[k, blocks].reshape(part_rows, share)
            cols = pl.ds(k * share, share)
            pre_gate += dot(x, w_gate[cols, :])
            pre_up += dot(x, w_up[cols, :])
            d_hid += dot(x, w_down[:, cols], ((1,), (1,)))
        d_hid = pltpu.roll(d_hid, part_rows - CAP, 0)
        sigma = 1.0 / (1.0 + jnp.exp(-pre_gate))
        silu = pre_gate * sigma
        d_up = d_hid * silu
        d_pre = d_hid * pre_up * sigma * (1.0 + pre_gate * (1.0 - sigma))
        twice_pre = jnp.where(is_token, d_pre, pltpu.roll(d_pre, CAP, 0)).astype(BF)
        twice_up = jnp.where(is_token, d_up, pltpu.roll(d_up, CAP, 0)).astype(BF)
        for k in range(TP):
            cols = pl.ds(k * share, share)
            grad = dot(twice_pre, w_gate[cols, :], ((1,), (1,)))
            grad += dot(twice_up, w_up[cols, :], ((1,), (1,)))
            folded = jnp.where(is_token, grad[:, :half_share], grad[:, half_share:])
            part[k, blocks] = folded.astype(BF).reshape(PLANE, ROWS, half_share)
        at = pl.ds(pl.multiple_of(plane * part_rows, part_rows), part_rows)
        d_both[at, 0:ff] = jnp.where(is_token, d_pre, 0.0).astype(BF)
        d_both[at, ff:] = jnp.where(is_token, d_up, 0.0).astype(BF)
        hid_rows[at, :] = jnp.where(is_token, 0.0, pltpu.roll(silu * pre_up, CAP, 0)).astype(BF)

    def far_half(g, k, to):
        at = plane_of(g, -1) * PLANE + k * mid
        return pltpu.make_async_remote_copy(
            part.at[far, pl.ds(at, mid)], near_in.at[k, g], a_out.at[k], a_in.at[k, g],
            device_id=device(me, to),
        )

    def near_sum(g, k, to):
        return pltpu.make_async_remote_copy(
            part.at[to, pl.ds(plane_of(g, -1) * PLANE, PLANE)], total_in.at[k, g], b_out.at[k],
            b_in.at[k, g], device_id=device(me, to),
        )

    def add(g, k, to):
        at = pl.ds(plane_of(g, -1) * PLANE + k * mid, mid)
        part[to, at] = (part[to, at].astype(F32) + near_in[k, g].astype(F32)).astype(BF)

    def send_back(g, j):
        to = plane_of(g, -1) * PLANE + (cell + j) % PLANE
        pltpu.make_async_remote_copy(
            sums.at[to], back.at[me], r_out, r_in, device_id=device(to, y)
        ).start()

    def step(t, c):
        @pl.when(t < PLANES)
        def _():
            wait_bytes(block(y, t), z_in.at[t])
            pass_on(y, t, 0, right).start()
            pass_on(y, t, 1, left).start()

        @pl.when((t > 1) & (t <= PLANES))
        def _():
            g = t - 1
            pass_on(left, g, 0, left).wait_recv()
            pass_on(left, g, 2, right).start()
            pass_on(right, g, 1, right).wait_recv()
            pass_on(right, g, 3, left).start()

        @pl.when((t >= 4) & (t < PLANES + 4))
        def _():
            g = t - 4
            far_half(g, 0, right).wait_recv()
            add(g, 0, right)
            far_half(g, 1, left).wait_recv()
            add(g, 1, left)

        @pl.when(t >= 5)
        def _():
            g = t - 5
            near_sum(g, 0, right).wait_recv()
            near_sum(g, 1, left).wait_recv()
            at = pl.ds(plane_of(g, -1) * PLANE, PLANE)
            sums[at] = (
                part[y, at].astype(F32) + total_in[0, g].astype(F32) + total_in[1, g].astype(F32)
            ).astype(BF)

        @pl.when((t >= 4) & (t < PLANES + 4))
        def _():
            near_sum(t - 4, 0, right).start()
            near_sum(t - 4, 1, left).start()

        @pl.when(t >= 5)
        def _():
            g = t - 5

            @pl.when(g > 0)
            def _():
                send_back(g, 0)

            lax.fori_loop(1, PLANE, lambda j, d: (send_back(g, j), d)[1], 0)

        @pl.when(t == 2)
        def _():
            wait_bytes(got.at[0, pl.ds(0, near)], f_in)

        @pl.when((t > 2) & (t < PLANES + 2))
        def _():
            pass_on(far, t - 2, 2, right).wait_recv()
            pass_on(far, t - 2, 3, left).wait_recv()

        @pl.when((t >= 2) & (t < PLANES + 2))
        def _():
            expert_rows(t - 2)
            far_half(t - 2, 0, right).start()
            far_half(t - 2, 1, left).start()

        return c

    lax.fori_loop(1, PLANES + 5, step, 0)
    back[me] = sums[me]

    wait_bytes(part.at[0, pl.ds(0, SP - 1)], r_in)
    token_slot = lax.broadcasted_iota(jnp.int32, (slots, 1), 0) % ROWS < CAP
    rows = back[...].reshape(slots, half_share)
    zero = jnp.zeros_like(rows)
    kept = jnp.concatenate(
        [jnp.where(token_slot, rows, zero), jnp.where(token_slot, zero, rows)], axis=1
    )
    total = (cot[:, mine].astype(F32) + dot(select[...], kept, ((0,), (0,)))).astype(BF)
    full[y] = total
    residual[...] = total

    def spread(s, k, to):
        ref = full.at[s] if k < 2 else full.at[s, pl.ds((k - 2) * (tokens // 2), tokens // 2)]
        return pltpu.make_async_remote_copy(
            ref, ref, e_out.at[k], e_in.at[k], device_id=device(me, to)
        )

    def weight_grads(k, c):
        rows = got[k].reshape(slots, share)
        at = pl.ds(pl.multiple_of(k * share, share), share)
        both = dot(rows, d_both[...], ((0,), (0,)))
        grad_gate[at, :] = both[:, :ff].astype(BF)
        grad_up[at, :] = both[:, ff:].astype(BF)
        grad_down[:, at] = dot(hid_rows[...], rows, ((0,), (0,))).astype(BF)
        return c

    sends = [spread(y, 0, right), spread(y, 1, left)]
    for copy in sends:
        copy.start()
    t_row = lax.broadcasted_iota(jnp.int32, (tokens, 1), 0)
    tap = [taps[i : i + 1, :].astype(F32) for i in range(3)]
    gated = c_gate[...].astype(F32) * x_in[...].astype(F32)
    edge_copy(0, 1).wait_recv()
    before = jnp.where(me == 0, 0.0, edge_in[0])
    one_back = jnp.where(t_row == 0, before[7:8], pltpu.roll(gated, 1, 0))
    two_back = jnp.where(
        t_row == 0, before[6:7], jnp.where(t_row == 1, before[7:8], pltpu.roll(gated, 2, 0))
    )
    conv = tap[0] * two_back + tap[1] * one_back + tap[2] * gated
    loads[7].wait()
    b_f = b_gate[...].astype(F32)
    y_short[...] = (b_f * conv).astype(BF)
    loads[8].wait()
    spread(left, 0, left).wait_recv()
    sends.append(spread(left, 2, right))
    sends[-1].start()
    spread(right, 1, right).wait_recv()
    sends.append(spread(right, 3, left))
    sends[-1].start()
    lax.fori_loop(0, 2, weight_grads, 0)
    spread(far, 2, right).wait_recv()
    spread(far, 3, left).wait_recv()

    for k in range(TP):
        grad = dot(full[k], y_short[...], ((0,), (0,))).astype(BF)
        for zz in range(2):
            for j in range(PLANE):
                at = (zz * PLANE + j) * 32
                outs[j, 2 * k + zz] = grad[at : at + 32]

    d_y = jnp.zeros((tokens, w_out.shape[1]), F32)
    for k in range(TP):
        d_y += dot(full[k], w_out[pl.ds(k * share, share), :])

    def send_out(j, c):
        to = (cell + j) % PLANE
        pltpu.make_async_remote_copy(
            outs.at[to], outs_in.at[cell], o_out, o_in, device_id=device(z * PLANE + to, y)
        ).start()
        return c

    lax.fori_loop(1, PLANE, send_out, 0)
    d_conv = b_f * d_y
    edge[1] = d_conv[0:8]
    grad_b[...] = (d_y * conv).astype(BF)
    edge_copy(1, -1).start()
    lax.fori_loop(2, 3, weight_grads, 0)
    edge_copy(1, -1).wait_recv()
    after = jnp.where(me == SP - 1, 0.0, edge_in[1])
    one_on = jnp.where(t_row == tokens - 1, after[0:1], pltpu.roll(d_conv, tokens - 1, 0))
    two_on = jnp.where(
        t_row == tokens - 2,
        after[0:1],
        jnp.where(t_row == tokens - 1, after[1:2], pltpu.roll(d_conv, tokens - 2, 0)),
    )
    d_v = tap[2] * d_conv + tap[1] * one_on + tap[0] * two_on
    grad_c[...] = (d_v * x_in[...].astype(F32)).astype(BF)
    grad_x[...] = (d_v * c_gate[...].astype(F32)).astype(BF)
    wait_bytes(outs_in.at[pl.ds(0, PLANE - 1)], o_in)

    def sum_plane(p, c):
        acc = outs[cell, p].astype(F32)
        for j in range(1, PLANE):
            acc += outs_in[(cell + j) % PLANE, p].astype(F32)
        plane_sum[p] = acc.astype(BF)
        return c

    lax.fori_loop(0, PLANES, sum_plane, 0)

    def send_sum(i, c):
        to = (z + i) % PLANES
        pltpu.make_async_remote_copy(
            plane_sum.at[to], plane_in.at[z], q_out, q_in, device_id=device(to * PLANE + cell, y)
        ).start()
        return c

    lax.fori_loop(1, PLANES, send_sum, 0)
    lax.fori_loop(3, 4, weight_grads, 0)
    wait_bytes(plane_in.at[pl.ds(0, PLANES - 1)], q_in)
    acc = plane_sum[z].astype(F32)
    for i in range(1, PLANES):
        acc += plane_in[(z + i) % PLANES].astype(F32)
    grad_out[...] = acc

    wait_bytes(got.at[0, pl.ds(0, SP - PLANE)], z_out)
    wait_bytes(got.at[0, pl.ds(0, near)], f_out)
    for k in range(4):
        size = PLANE if k < 2 else mid
        wait_bytes(got.at[0, pl.ds(0, size * (PLANES - 1))], y_out.at[k])
    for k in range(2):
        wait_bytes(part.at[0, pl.ds(0, SP // 2)], a_out.at[k])
        wait_bytes(part.at[0], b_out.at[k])
        edge_copy(k, 1).wait_send()
    wait_bytes(part.at[0, pl.ds(0, SP - 1)], r_out)
    for copy in sends:
        copy.wait_send()
    wait_bytes(outs_in.at[pl.ds(0, PLANE - 1)], o_out)
    wait_bytes(plane_in.at[pl.ds(0, PLANES - 1)], q_out)


def per_device(
    hidden_in, cotangent, routes, routing_weights, w_gate, w_up, w_down, b_gate, c_gate, x_in, taps, w_out
):
    tokens, width = hidden_in.shape
    share, ff, short = width // TP, w_gate.shape[2], x_in.shape[1]
    half = share // 2
    slots, out_rows = SP * ROWS, width // SP
    like, dma = jax.ShapeDtypeStruct, pltpu.SemaphoreType.DMA
    hbm = pl.BlockSpec(memory_space=pl.ANY)
    outs = pl.pallas_call(
        kernel,
        out_shape=(
            like((width, ff), BF),
            like((width, ff), BF),
            like((ff, width), BF),
            like((out_rows, short), F32),
            like((tokens, share), BF),
            like((tokens, short), BF),
            like((tokens, short), BF),
            like((tokens, short), BF),
        ),
        in_specs=[VMEM] * 3 + [hbm] * 9,
        out_specs=(VMEM,) * 8,
        scratch_shapes=[
            pltpu.VMEM((tokens, width), BF),
            pltpu.VMEM((tokens, width), BF),
            pltpu.VMEM((width, ff), BF),
            pltpu.VMEM((width, ff), BF),
            pltpu.VMEM((ff, width), BF),
            pltpu.VMEM((width, short), BF),
            pltpu.VMEM((tokens, short), BF),
            pltpu.VMEM((tokens, short), BF),
            pltpu.VMEM((tokens, short), BF),
            pltpu.VMEM((SP, ROWS, share), BF),
            pltpu.VMEM((TP, PLANE, ROWS, share), BF),
            pltpu.VMEM((slots, tokens), BF),
            pltpu.VMEM((TP, SP, ROWS, share), BF),
            pltpu.VMEM((TP, SP, ROWS, half), BF),
            pltpu.VMEM((2, PLANES, PLANE // 2, ROWS, half), BF),
            pltpu.VMEM((2, PLANES, PLANE, ROWS, half), BF),
            pltpu.VMEM((SP, ROWS, half), BF),
            pltpu.VMEM((SP, ROWS, half), BF),
            pltpu.VMEM((slots, 2 * ff), BF),
            pltpu.VMEM((slots, ff), BF),
            pltpu.VMEM((TP, tokens, share), BF),
            pltpu.VMEM((tokens, short), BF),
            pltpu.VMEM((2, 8, short), F32),
            pltpu.VMEM((2, 8, short), F32),
            pltpu.VMEM((PLANE, PLANES, out_rows, short), BF),
            pltpu.VMEM((PLANE, PLANES, out_rows, short), BF),
            pltpu.VMEM((PLANES, out_rows, short), BF),
            pltpu.VMEM((PLANES, out_rows, short), BF),
            dma((9,)),
            dma((PLANES,)),
            dma(()),
            dma(()),
            dma(()),
            dma((4, PLANES)),
            dma((4,)),
            dma((2, PLANES)),
            dma((2,)),
            dma((2, PLANES)),
            dma((2,)),
            dma(()),
            dma(()),
            dma((2,)),
            dma((2,)),
            dma((4,)),
            dma((4,)),
            dma(()),
            dma(()),
            dma(()),
            dma(()),
        ],
        compiler_params=pltpu.CompilerParams(
            collective_id=0, has_side_effects=True, vmem_limit_bytes=62 * 2**20
        ),
        name="layer",
    )(
        routes.T, routing_weights.T, taps, hidden_in, cotangent, w_gate[0], w_up[0], w_down[0], w_out,
        b_gate, c_gate, x_in,
    )
    grad_gate, grad_up, grad_down, grad_out, residual, grad_b, grad_c, grad_x = outs
    return grad_gate[None], grad_up[None], grad_down[None], grad_out, residual, grad_b, grad_c, grad_x


def solution(mesh):
    seq, both = P("sp", None), P("sp", "tp")
    return jax.shard_map(
        per_device,
        mesh=mesh,
        in_specs=(
            seq,
            seq,
            seq,
            seq,
            P("sp", None, "tp"),
            P("sp", None, "tp"),
            P("sp", "tp", None),
            both,
            both,
            both,
            P(None, "tp"),
            P(None, "tp"),
        ),
        out_specs=(
            P("sp", None, "tp"),
            P("sp", None, "tp"),
            P("sp", "tp", None),
            both,
            both,
            both,
            both,
            both,
        ),
        check_vma=False,
    )
```

time: 340 us -> 159 us (0.47)
  Pallas kernels: 0 us -> 149 us
  waiting for transfers between devices: 112 us -> 0 us
  blocking collectives: 102 us -> 0 us
  local copies, waits for them, and re-layouts: 40.7 us -> 9.1 us
  starting transfers between devices: 28.6 us -> 0 us
  matrix products: 25.4 us -> 0 us
  other arithmetic: 15.7 us -> 0 us
  between operations: 14.6 us -> 0.66 us
    pallas_call x0 -> x1, Pallas kernels: none -> 149 us  [per_device(): pl.pallas_call(kernel, out_shape=(like((width, ff), BF), like((width, ff)...]
    all_to_all x2 -> x0, blocking collectives: 102 us -> none  [the longest x1 62.5 us: in_one_piece(): lax.all_to_all(both, axis, split_axis=split_dim, concat_axis=concat_dim,...]
    all_gather x1 -> x0, waiting for transfers between devices: 66 us -> none  [sent_together(): lax.all_gather(both, axis, axis=dim, tiled=True)]
    all_to_all x3 -> x0, waiting for transfers between devices: 44.9 us -> none  [the longest x1 23 us: per_device(): lax.all_to_all(shared_rows, 'sp', split_axis=1, concat_axis=0, tiled=True)]
    dot_general x10 -> x0, matrix products: 25.4 us -> none  [the longest x1 4.02 us: per_device(): jnp.einsum('erd,erf->edf', rows_h, d_pre, preferred_element_type=jnp.floa...]
    all_to_all x3 -> x0, starting transfers between devices: 22.3 us -> none  [the longest x1 12 us: per_device(): lax.all_to_all(shared_rows, 'sp', split_axis=1, concat_axis=0, tiled=True)]
    gather x5 -> x0, local copies, waits for them, and re-layouts: 15.7 us -> none  [the longest x2 5.42 us: per_device(): rows_src[token_of]]
    ppermute x2 -> x0, starting transfers between devices: 6.17 us -> none  [from_behind(): return lax.ppermute(x, axis, pairs)]
  transfers between devices with their start and end apart: 6 -> 0, of which waited for: 5 -> 0; matrix products, arithmetic and copies ran while one was open for 4% -> 0% of each run, Pallas kernels for 0% -> 0%
where the time goes in v2:
time: 159 us; the launch traced here: 158 us
  Pallas kernels  149 us (94%)
  local copies, waits for them, and re-layouts  9.1 us (6%)
    pallas_call x1, Pallas kernels, per_device(): pl.pallas_call(kernel, out_shape=(like((width, ff), BF), like((width, ff)...  149 us
    unnamed x22, local copies, waits for them, and re-layouts  9.1 us

profile of v2, /device:TPU:1, one launch (start us, length us, event | category | flops | bytes accessed | tf_op | source)
XLA Modules:
  0.0 158.5 jit_solution(16122933921418634814)
XLA Ops:
  0.6 148.7 %layer.1 = (bf16[2048,256]{1,0:T(8,128)(2,1)}, bf16[2048,256]{1,0:T(8,128)(2,1)}, bf16[256,2048]{1,0:T(8,128)(2,1)}, f32[32,256]{1,0:T(8,128)}, bf16[256,512]{1,...) custom-call(s32[2,256]{1,0:T(2,128)} %bitcast.14, ...), custom_call_target="tpu_custom_call" | custom-call | tf_op jit(solution)/shard_map/layer/pallas_call | solution.py:445
  149.3 0.0 copy-start.1
  149.3 2.4 %copy.28 = bf16[1,2048,256]{2,1,0:T(8,128)(2,1)} copy(bf16[1,2048,256]{2,1,0:T(8,128)(2,1)} %bitcast.10) | data formatting | bytes 2097152
  151.7 0.0 copy-done.1
  151.7 0.0 copy-start
  151.7 1.0 copy.29
  152.7 0.6 copy-done
  153.3 0.0 copy-start.6
  153.3 0.0 copy-start.2
  153.3 1.0 copy.30
  154.3 0.0 copy-done.6
  154.3 0.6 copy.31
  154.9 0.0 copy-done.2
  154.9 0.0 copy-start.5
  154.9 0.7 copy.32
  155.6 0.3 copy-done.5
  155.9 0.0 copy-start.4
  155.9 0.7 copy.33
  156.6 0.3 copy-done.4
  156.9 0.0 copy-start.3
  156.9 0.7 copy.34
  157.5 0.3 copy-done.3
  157.8 0.7 copy.35
Async XLA Ops:
  149.3 2.4 %copy-start.1 = (bf16[2048,256]{1,0:T(8,128)(2,1)S(1)}, bf16[2048,256]{1,0:T(8,128)(2,1)}, u32[]{:S(2)}) copy-start(bf16[2048,256]{1,0:T(8,128)(2,1)} %get-tuple-element.17) | copy-start | bytes 3145732
  151.7 1.6 %copy-start = (bf16[256,2048]{1,0:T(8,128)(2,1)S(1)}, bf16[256,2048]{1,0:T(8,128)(2,1)}, u32[]{:S(2)}) copy-start(bf16[256,2048]{1,0:T(8,128)(2,1)} %get-tuple-element.18) | copy-start | bytes 3145732
  153.3 1.0 copy-start.6
  153.3 1.6 %copy-start.2 = (bf16[256,512]{1,0:T(8,128)(2,1)S(1)}, bf16[256,512]{1,0:T(8,128)(2,1)}, u32[]{:S(2)}) copy-start(bf16[256,512]{1,0:T(8,128)(2,1)} %get-tuple-element.36) | copy-start | bytes 786436
  154.9 1.0 copy-start.5
  155.9 1.0 copy-start.4
  156.9 1.0 copy-start.3

commit v3 on v2

--- a/solution.py
+++ b/solution.py
@@ -22,8 +22,16 @@
     return {"sp": sp, "tp": tp}
 
 
+STEPS = (0, 2, 6, 3, 5, 4, 1, 7)
+NEAR = (0, 6, 7)
+FAR = range(1, 6)
+NEAR_AT = 3
+
+
 def plane_step(g):
-    return ((g + 1) // 2) * (2 * (g % 2) - 1)
+    if isinstance(g, int):
+        return STEPS[g]
+    return sum(jnp.where(g == i, step, 0) for i, step in enumerate(STEPS))
 
 
 def greet_all(me, y, right, left):
@@ -62,6 +70,7 @@
     slots = SP * ROWS
     mid = PLANE // 2
     ff = w_gate.shape[1]
+    out_rows = grad_out.shape[0]
 
     loads = [
         pltpu.make_async_copy(a, b, ld.at[i])
@@ -131,40 +140,41 @@
 
     loads[0].wait()
     loads[1].wait()
-    pack(1)
+    def pack_full(n):
+        plane = plane_of(NEAR[n], 1)
+        h, s, scale = picks(plane)
+        for k in range(TP):
+            cols = pl.ds(k * share, share)
+            rows = (dot(h, hidden[:, cols]) + dot(s, cot[:, cols])) * scale
+            own[n, k] = rows.astype(BF).reshape(PLANE, ROWS, share)
+
+    def send_full(n, first):
+        count = PLANE - first
+
+        def one(i, c):
+            j, k = (cell + first + i % count) % PLANE, i // count
+            to = plane_of(NEAR[n], 1) * PLANE + j
+            pltpu.make_async_remote_copy(
+                own.at[n, k, j], got.at[k, me], f_out.at[n], f_in.at[n], device_id=device(to, y)
+            ).start()
+            return c
+
+        lax.fori_loop(0, TP * count, one, 0)
+
+    lax.fori_loop(FAR[0], FAR[-1] + 1, lambda g, c: (pack(g), c)[1], 0)
+    pack_full(0)
+    for k in range(TP):
+        got[k, me] = own[0, k, cell]
     pl.semaphore_wait(barrier, SP + 1)
-
-    def pack_ahead(g, c):
-        pack(g + 1)
-        send_group(g)
-        return c
-
-    lax.fori_loop(1, 3, pack_ahead, 0)
-    h, s, scale = picks(z)
-    for k in range(TP):
-        cols = pl.ds(k * share, share)
-        rows = (dot(h, hidden[:, cols]) + dot(s, cot[:, cols])) * scale
-        own[k] = rows.astype(BF).reshape(PLANE, ROWS, share)
-    send_group(3)
-    for k in range(TP):
-        got[k, me] = own[k, cell]
-
-    def send_full(i, c):
-        j, k = (cell + 1 + i % (PLANE - 1)) % PLANE, i // (PLANE - 1)
-        pltpu.make_async_remote_copy(
-            own.at[k, j], got.at[k, me], f_out, f_in, device_id=device(z * PLANE + j, y)
-        ).start()
-        return c
-
-    near = TP * (PLANE - 1)
-    lax.fori_loop(0, near, send_full, 0)
-    pack(4)
-    lax.fori_loop(4, PLANES - 1, pack_ahead, 0)
+    lax.fori_loop(1, 3, lambda g, c: (send_group(g), c)[1], 0)
+    send_full(0, 1)
+    lax.fori_loop(3, FAR[-1] + 1, lambda g, c: (send_group(g), c)[1], 0)
+    pack_full(1)
+    pack_full(2)
 
     loads[2].wait()
     loads[3].wait()
     edge[0] = c_gate[tokens - 8 :, :].astype(F32) * x_in[tokens - 8 :, :].astype(F32)
-    send_group(PLANES - 1)
 
     def edge_copy(k, by):
         return pltpu.make_async_remote_copy(
@@ -235,14 +245,22 @@
             sums.at[to], back.at[me], r_out, r_in, device_id=device(to, y)
         ).start()
 
+    def full_blocks(n):
+        return got.at[0, pl.ds(0, TP * (PLANE - 1 if n == 0 else PLANE))]
+
     def step(t, c):
-        @pl.when(t < PLANES)
+        @pl.when(t == NEAR_AT)
+        def _():
+            send_full(1, 0)
+            send_full(2, 0)
+
+        @pl.when(t <= FAR[-1])
         def _():
             wait_bytes(block(y, t), z_in.at[t])
             pass_on(y, t, 0, right).start()
             pass_on(y, t, 1, left).start()
 
-        @pl.when((t > 1) & (t <= PLANES))
+        @pl.when((t > 1) & (t <= FAR[-1] + 1))
         def _():
             g = t - 1
             pass_on(left, g, 0, left).wait_recv()
@@ -258,7 +276,22 @@
             far_half(g, 1, left).wait_recv()
             add(g, 1, left)
 
-        @pl.when(t >= 5)
+        @pl.when(t >= 6)
+        def _():
+            g = t - 6
+
+            @pl.when(g > 0)
+            def _():
+                send_back(g, 0)
+
+            lax.fori_loop(1, PLANE, lambda j, d: (send_back(g, j), d)[1], 0)
+
+        @pl.when((t >= 4) & (t < PLANES + 4))
+        def _():
+            near_sum(t - 4, 0, right).start()
+            near_sum(t - 4, 1, left).start()
+
+        @pl.when((t >= 5) & (t < PLANES + 5))
         def _():
             g = t - 5
             near_sum(g, 0, right).wait_recv()
@@ -268,26 +301,13 @@
                 part[y, at].astype(F32) + total_in[0, g].astype(F32) + total_in[1, g].astype(F32)
             ).astype(BF)
 
-        @pl.when((t >= 4) & (t < PLANES + 4))
-        def _():
-            near_sum(t - 4, 0, right).start()
-            near_sum(t - 4, 1, left).start()
-
-        @pl.when(t >= 5)
-        def _():
-            g = t - 5
-
-            @pl.when(g > 0)
+        for n, g in enumerate(NEAR):
+
+            @pl.when(t == g + 2)
             def _():
-                send_back(g, 0)
-
-            lax.fori_loop(1, PLANE, lambda j, d: (send_back(g, j), d)[1], 0)
-
-        @pl.when(t == 2)
-        def _():
-            wait_bytes(got.at[0, pl.ds(0, near)], f_in)
-
-        @pl.when((t > 2) & (t < PLANES + 2))
+                wait_bytes(full_blocks(n), f_in.at[n])
+
+        @pl.when((t > 2) & (t <= FAR[-1] + 2))
         def _():
             pass_on(far, t - 2, 2, right).wait_recv()
             pass_on(far, t - 2, 3, left).wait_recv()
@@ -300,7 +320,7 @@
 
         return c
 
-    lax.fori_loop(1, PLANES + 5, step, 0)
+    lax.fori_loop(1, PLANES + 6, step, 0)
     back[me] = sums[me]
 
     wait_bytes(part.at[0, pl.ds(0, SP - 1)], r_in)
@@ -314,8 +334,10 @@
     full[y] = total
     residual[...] = total
 
-    def spread(s, k, to):
-        ref = full.at[s] if k < 2 else full.at[s, pl.ds((k - 2) * (tokens // 2), tokens // 2)]
+    rows_half = tokens // 2
+
+    def spread(s, at, k, to):
+        ref = full.at[s, pl.ds(at * rows_half, rows_half)]
         return pltpu.make_async_remote_copy(
             ref, ref, e_out.at[k], e_in.at[k], device_id=device(me, to)
         )
@@ -329,7 +351,7 @@
         grad_down[:, at] = dot(hid_rows[...], rows, ((0,), (0,))).astype(BF)
         return c
 
-    sends = [spread(y, 0, right), spread(y, 1, left)]
+    sends = [spread(y, 0, 0, right), spread(y, 1, 1, left), spread(y, 1, 2, right), spread(y, 0, 3, left)]
     for copy in sends:
         copy.start()
     t_row = lax.broadcasted_iota(jnp.int32, (tokens, 1), 0)
@@ -346,39 +368,53 @@
     b_f = b_gate[...].astype(F32)
     y_short[...] = (b_f * conv).astype(BF)
     loads[8].wait()
-    spread(left, 0, left).wait_recv()
-    sends.append(spread(left, 2, right))
-    sends[-1].start()
-    spread(right, 1, right).wait_recv()
-    sends.append(spread(right, 3, left))
-    sends[-1].start()
-    lax.fori_loop(0, 2, weight_grads, 0)
-    spread(far, 2, right).wait_recv()
-    spread(far, 3, left).wait_recv()
-
-    for k in range(TP):
+
+    def project(k):
         grad = dot(full[k], y_short[...], ((0,), (0,))).astype(BF)
         for zz in range(2):
             for j in range(PLANE):
-                at = (zz * PLANE + j) * 32
-                outs[j, 2 * k + zz] = grad[at : at + 32]
-
-    d_y = jnp.zeros((tokens, w_out.shape[1]), F32)
-    for k in range(TP):
-        d_y += dot(full[k], w_out[pl.ds(k * share, share), :])
-
-    def send_out(j, c):
-        to = (cell + j) % PLANE
-        pltpu.make_async_remote_copy(
-            outs.at[to], outs_in.at[cell], o_out, o_in, device_id=device(z * PLANE + to, y)
-        ).start()
-        return c
-
-    lax.fori_loop(1, PLANE, send_out, 0)
+                at = (zz * PLANE + j) * out_rows
+                outs[j, 2 * k + zz] = grad[at : at + out_rows]
+        return dot(full[k], w_out[pl.ds(pl.multiple_of(k * share, share), share), :])
+
+    def send_out(k):
+        def one(j, c):
+            to = (cell + j) % PLANE
+            pltpu.make_async_remote_copy(
+                outs.at[to, pl.ds(2 * k, 2)],
+                outs_in.at[cell, pl.ds(2 * k, 2)],
+                o_out,
+                o_in,
+                device_id=device(z * PLANE + to, y),
+            ).start()
+            return c
+
+        lax.fori_loop(1, PLANE, one, 0)
+
+    d_y = project(y)
+    send_out(y)
+    lax.fori_loop(0, 1, weight_grads, 0)
+    spread(left, 0, 0, left).wait_recv()
+    sends.append(spread(left, 0, 4, right))
+    sends[-1].start()
+    spread(right, 1, 1, right).wait_recv()
+    sends.append(spread(right, 1, 5, left))
+    sends[-1].start()
+    spread(left, 1, 2, left).wait_recv()
+    d_y += project(left)
+    send_out(left)
+    spread(right, 0, 3, right).wait_recv()
+    d_y += project(right)
+    send_out(right)
+    lax.fori_loop(1, 2, weight_grads, 0)
+    spread(far, 0, 4, right).wait_recv()
+    spread(far, 1, 5, left).wait_recv()
+    d_y += project(far)
     d_conv = b_f * d_y
     edge[1] = d_conv[0:8]
     grad_b[...] = (d_y * conv).astype(BF)
     edge_copy(1, -1).start()
+    send_out(far)
     lax.fori_loop(2, 3, weight_grads, 0)
     edge_copy(1, -1).wait_recv()
     after = jnp.where(me == SP - 1, 0.0, edge_in[1])
@@ -417,11 +453,11 @@
         acc += plane_in[(z + i) % PLANES].astype(F32)
     grad_out[...] = acc
 
-    wait_bytes(got.at[0, pl.ds(0, SP - PLANE)], z_out)
-    wait_bytes(got.at[0, pl.ds(0, near)], f_out)
+    wait_bytes(got.at[0, pl.ds(0, len(FAR) * PLANE)], z_out)
+    for n in range(len(NEAR)):
+        wait_bytes(full_blocks(n), f_out.at[n])
     for k in range(4):
-        size = PLANE if k < 2 else mid
-        wait_bytes(got.at[0, pl.ds(0, size * (PLANES - 1))], y_out.at[k])
+        wait_bytes(got.at[0, pl.ds(0, (PLANE if k < 2 else mid) * len(FAR))], y_out.at[k])
     for k in range(2):
         wait_bytes(part.at[0, pl.ds(0, SP // 2)], a_out.at[k])
         wait_bytes(part.at[0], b_out.at[k])
@@ -467,7 +503,7 @@
             pltpu.VMEM((tokens, short), BF),
             pltpu.VMEM((tokens, short), BF),
             pltpu.VMEM((SP, ROWS, share), BF),
-            pltpu.VMEM((TP, PLANE, ROWS, share), BF),
+            pltpu.VMEM((len(NEAR), TP, PLANE, ROWS, share), BF),
             pltpu.VMEM((slots, tokens), BF),
             pltpu.VMEM((TP, SP, ROWS, share), BF),
             pltpu.VMEM((TP, SP, ROWS, half), BF),
@@ -488,8 +524,8 @@
             dma((9,)),
             dma((PLANES,)),
             dma(()),
-            dma(()),
-            dma(()),
+            dma((len(NEAR),)),
+            dma((len(NEAR),)),
             dma((4, PLANES)),
             dma((4,)),
             dma((2, PLANES)),
@@ -500,20 +536,23 @@
             dma(()),
             dma((2,)),
             dma((2,)),
-            dma((4,)),
-            dma((4,)),
+            dma((6,)),
+            dma((6,)),
             dma(()),
             dma(()),
             dma(()),
             dma(()),
         ],
         compiler_params=pltpu.CompilerParams(
-            collective_id=0, has_side_effects=True, vmem_limit_bytes=62 * 2**20
+            collective_id=0, has_side_effects=True, vmem_limit_bytes=44 * 2**20
         ),
         name="layer",
     )(
-        routes.T, routing_weights.T, taps, hidden_in, cotangent, w_gate[0], w_up[0], w_down[0], w_out,
-        b_gate, c_gate, x_in,
+        routes.T, routing_weights.T, taps,
+        *[
+            pltpu.with_memory_space_constraint(v, pltpu.HBM)
+            for v in (hidden_in, cotangent, w_gate[0], w_up[0], w_down[0], w_out, b_gate, c_gate, x_in)
+        ],
     )
     grad_gate, grad_up, grad_down, grad_out, residual, grad_b, grad_c, grad_x = outs
     return grad_gate[None], grad_up[None], grad_down[None], grad_out, residual, grad_b, grad_c, grad_x

time: 159 us -> 131 us (0.82)
  Pallas kernels: 149 us -> 123 us
  local copies, waits for them, and re-layouts: 9.1 us -> 6.88 us
    pallas_call x1, Pallas kernels: 149 us -> 123 us  [per_device(): pl.pallas_call(kernel, out_shape=(like((width, ff), BF), like((width, ff)...]
    unnamed x22 -> x14, local copies, waits for them, and re-layouts: 9.1 us -> 6.88 us
where the time goes in v3:
time: 131 us
  Pallas kernels  123 us (94%)
  local copies, waits for them, and re-layouts  6.88 us (5%)
    pallas_call x1, Pallas kernels, per_device(): pl.pallas_call(kernel, out_shape=(like((width, ff), BF), like((width, ff)...  123 us
    unnamed x14, local copies, waits for them, and re-layouts  6.88 us

profile of v3, /device:TPU:1, one launch (start us, length us, event | category | flops | bytes accessed | tf_op | source)
XLA Modules:
  0.0 131.0 jit_solution(8362294576378082740)
XLA Ops:
  0.6 0.0 copy-start.2
  0.6 0.0 copy-start.1
  0.7 0.0 copy-start
  0.7 0.7 copy-done.2
  1.3 0.0 copy-done.1
  1.3 0.0 copy-done
  1.4 123.4 %layer.1 = (bf16[2048,256]{1,0:T(8,128)(2,1)S(1)}, bf16[2048,256]{1,0:T(8,128)(2,1)S(1)}, bf16[256,2048]{1,0:T(8,128)(2,1)S(1)}, f32[32,256]{1,0:T(8,128)S(1)}, ...) custom-call(s32[2,256]{1,0:T(2,128)S(1)} %bitcast.11, ...), custom_call_target="tpu_custom_call" | custom-call | tf_op jit(solution)/shard_map/layer/pallas_call | solution.py:481
  124.8 1.0 copy.28
  125.8 1.0 copy.29
  126.7 1.0 copy.30
  127.7 0.6 copy.31
  128.3 0.7 copy.32
  129.0 0.7 copy.33
  129.7 0.7 copy.34
  130.3 0.7 copy.35
Async XLA Ops:
  0.6 0.7 copy-start.2
  0.6 0.7 copy-start.1
  0.7 0.7 copy-start

commit v4 on v3

--- a/solution.py
+++ b/solution.py
@@ -53,12 +53,12 @@
 
 def kernel(
     routes, weights, taps, hidden_hbm, cot_hbm, w_gate_hbm, w_up_hbm, w_down_hbm, w_out_hbm, b_hbm, c_hbm, x_hbm,
-    grad_gate, grad_up, grad_down, grad_out, residual, grad_b, grad_c, grad_x,
+    grad_gate, grad_up, grad_down, grad_out, residual, small,
     hidden, cot, w_gate, w_up, w_down, w_out, b_gate, c_gate, x_in,
     send, own, select, got, part, near_in, total_in, sums, back, d_both, hid_rows, full, y_short,
-    edge, edge_in, outs, outs_in, plane_sum, plane_in,
+    edge, edge_in, outs, pair_in, pair_sum, outs_in, plane_sum, plane_in,
     ld, z_in, z_out, f_in, f_out, y_in, y_out, a_in, a_out, b_in, b_out, r_in, r_out,
-    h_in, h_out, e_in, e_out, o_in, o_out, q_in, q_out,
+    h_in, h_out, e_in, e_out, p_in, p_out, o_in, o_out, q_in, q_out,
 ):
     me, y = lax.axis_index("sp"), lax.axis_index("tp")
     z, cell = me // PLANE, me % PLANE
@@ -72,6 +72,7 @@
     ff = w_gate.shape[1]
     out_rows = grad_out.shape[0]
 
+    barrier = greet_all(me, y, right, left)
     loads = [
         pltpu.make_async_copy(a, b, ld.at[i])
         for i, (a, b) in enumerate(
@@ -90,7 +91,6 @@
     ]
     for load in loads:
         load.start()
-    barrier = greet_all(me, y, right, left)
 
     down = lax.broadcasted_iota(jnp.int32, (tokens, tokens), 0)
     across = lax.broadcasted_iota(jnp.int32, (tokens, tokens), 1)
@@ -161,14 +161,15 @@
 
         lax.fori_loop(0, TP * count, one, 0)
 
-    lax.fori_loop(FAR[0], FAR[-1] + 1, lambda g, c: (pack(g), c)[1], 0)
+    lax.fori_loop(1, 3, lambda g, c: (pack(g), c)[1], 0)
+    pl.semaphore_wait(barrier, SP + 1)
+    lax.fori_loop(1, 3, lambda g, c: (send_group(g), c)[1], 0)
+    lax.fori_loop(3, FAR[-1] + 1, lambda g, c: (pack(g), c)[1], 0)
     pack_full(0)
     for k in range(TP):
         got[k, me] = own[0, k, cell]
-    pl.semaphore_wait(barrier, SP + 1)
-    lax.fori_loop(1, 3, lambda g, c: (send_group(g), c)[1], 0)
+    lax.fori_loop(3, FAR[-1] + 1, lambda g, c: (send_group(g), c)[1], 0)
     send_full(0, 1)
-    lax.fori_loop(3, FAR[-1] + 1, lambda g, c: (send_group(g), c)[1], 0)
     pack_full(1)
     pack_full(2)
 
@@ -374,26 +375,33 @@
         for zz in range(2):
             for j in range(PLANE):
                 at = (zz * PLANE + j) * out_rows
-                outs[j, 2 * k + zz] = grad[at : at + out_rows]
+                outs[j % 2, j // 2, 2 * k + zz] = grad[at : at + out_rows]
         return dot(full[k], w_out[pl.ds(pl.multiple_of(k * share, share), share), :])
 
+    core, x_at = cell % 2, cell // 2
+    chips = PLANE // 2
+
+    def to_partner(k):
+        return pltpu.make_async_remote_copy(
+            outs.at[1 - core, :, pl.ds(2 * k, 2)], pair_in.at[:, pl.ds(2 * k, 2)], p_out.at[k], p_in.at[k],
+            device_id=device(z * PLANE + x_at * 2 + 1 - core, y),
+        )
+
     def send_out(k):
-        def one(j, c):
-            to = (cell + j) % PLANE
+        to_partner(k).wait_recv()
+        at = pl.ds(2 * k, 2)
+        pair_sum[:, at] = (outs[core, :, at].astype(F32) + pair_in[:, at].astype(F32)).astype(BF)
+        for j in range(1, chips):
+            to = (x_at + j) % chips
             pltpu.make_async_remote_copy(
-                outs.at[to, pl.ds(2 * k, 2)],
-                outs_in.at[cell, pl.ds(2 * k, 2)],
-                o_out,
-                o_in,
-                device_id=device(z * PLANE + to, y),
+                pair_sum.at[to, at], outs_in.at[x_at, at], o_out, o_in,
+                device_id=device(z * PLANE + to * 2 + core, y),
             ).start()
-            return c
-
-        lax.fori_loop(1, PLANE, one, 0)
 
     d_y = project(y)
+    to_partner(y).start()
+    lax.fori_loop(0, 1, weight_grads, 0)
     send_out(y)
-    lax.fori_loop(0, 1, weight_grads, 0)
     spread(left, 0, 0, left).wait_recv()
     sends.append(spread(left, 0, 4, right))
     sends[-1].start()
@@ -402,17 +410,20 @@
     sends[-1].start()
     spread(left, 1, 2, left).wait_recv()
     d_y += project(left)
-    send_out(left)
+    to_partner(left).start()
     spread(right, 0, 3, right).wait_recv()
     d_y += project(right)
+    to_partner(right).start()
+    send_out(left)
     send_out(right)
     lax.fori_loop(1, 2, weight_grads, 0)
     spread(far, 0, 4, right).wait_recv()
     spread(far, 1, 5, left).wait_recv()
     d_y += project(far)
+    to_partner(far).start()
     d_conv = b_f * d_y
     edge[1] = d_conv[0:8]
-    grad_b[...] = (d_y * conv).astype(BF)
+    small[0] = (d_y * conv).astype(BF)
     edge_copy(1, -1).start()
     send_out(far)
     lax.fori_loop(2, 3, weight_grads, 0)
@@ -425,14 +436,14 @@
         jnp.where(t_row == tokens - 1, after[1:2], pltpu.roll(d_conv, tokens - 2, 0)),
     )
     d_v = tap[2] * d_conv + tap[1] * one_on + tap[0] * two_on
-    grad_c[...] = (d_v * x_in[...].astype(F32)).astype(BF)
-    grad_x[...] = (d_v * c_gate[...].astype(F32)).astype(BF)
-    wait_bytes(outs_in.at[pl.ds(0, PLANE - 1)], o_in)
+    small[1] = (d_v * x_in[...].astype(F32)).astype(BF)
+    small[2] = (d_v * c_gate[...].astype(F32)).astype(BF)
+    wait_bytes(outs_in.at[pl.ds(0, chips - 1)], o_in)
 
     def sum_plane(p, c):
-        acc = outs[cell, p].astype(F32)
-        for j in range(1, PLANE):
-            acc += outs_in[(cell + j) % PLANE, p].astype(F32)
+        acc = pair_sum[x_at, p].astype(F32)
+        for j in range(1, chips):
+            acc += outs_in[(x_at + j) % chips, p].astype(F32)
         plane_sum[p] = acc.astype(BF)
         return c
 
@@ -465,7 +476,9 @@
     wait_bytes(part.at[0, pl.ds(0, SP - 1)], r_out)
     for copy in sends:
         copy.wait_send()
-    wait_bytes(outs_in.at[pl.ds(0, PLANE - 1)], o_out)
+    wait_bytes(outs_in.at[pl.ds(0, chips - 1)], o_out)
+    for k in range(TP):
+        to_partner(k).wait_send()
     wait_bytes(plane_in.at[pl.ds(0, PLANES - 1)], q_out)
 
 
@@ -486,12 +499,10 @@
             like((ff, width), BF),
             like((out_rows, short), F32),
             like((tokens, share), BF),
-            like((tokens, short), BF),
-            like((tokens, short), BF),
-            like((tokens, short), BF),
+            like((3, tokens, short), BF),
         ),
         in_specs=[VMEM] * 3 + [hbm] * 9,
-        out_specs=(VMEM,) * 8,
+        out_specs=(VMEM,) * 6,
         scratch_shapes=[
             pltpu.VMEM((tokens, width), BF),
             pltpu.VMEM((tokens, width), BF),
@@ -517,8 +528,10 @@
             pltpu.VMEM((tokens, short), BF),
             pltpu.VMEM((2, 8, short), F32),
             pltpu.VMEM((2, 8, short), F32),
-            pltpu.VMEM((PLANE, PLANES, out_rows, short), BF),
-            pltpu.VMEM((PLANE, PLANES, out_rows, short), BF),
+            pltpu.VMEM((2, PLANE // 2, PLANES, out_rows, short), BF),
+            pltpu.VMEM((PLANE // 2, PLANES, out_rows, short), BF),
+            pltpu.VMEM((PLANE // 2, PLANES, out_rows, short), BF),
+            pltpu.VMEM((PLANE // 2, PLANES, out_rows, short), BF),
             pltpu.VMEM((PLANES, out_rows, short), BF),
             pltpu.VMEM((PLANES, out_rows, short), BF),
             dma((9,)),
@@ -538,6 +551,8 @@
             dma((2,)),
             dma((6,)),
             dma((6,)),
+            dma((TP,)),
+            dma((TP,)),
             dma(()),
             dma(()),
             dma(()),
@@ -554,7 +569,8 @@
             for v in (hidden_in, cotangent, w_gate[0], w_up[0], w_down[0], w_out, b_gate, c_gate, x_in)
         ],
     )
-    grad_gate, grad_up, grad_down, grad_out, residual, grad_b, grad_c, grad_x = outs
+    grad_gate, grad_up, grad_down, grad_out, residual, small = outs
+    grad_b, grad_c, grad_x = small[0], small[1], small[2]
     return grad_gate[None], grad_up[None], grad_down[None], grad_out, residual, grad_b, grad_c, grad_x
 
 

time: 131 us -> 125 us (0.954)
  Pallas kernels: 123 us -> 118 us
    pallas_call x1, Pallas kernels: 123 us -> 118 us  [per_device(): pl.pallas_call(kernel, out_shape=(like((width, ff), BF), like((width, ff)...]
    unnamed x14 -> x11, local copies, waits for them, and re-layouts: 6.88 us -> 4.91 us
where the time goes in v4:
time: 125 us; the launch traced here: 124 us
  Pallas kernels  118 us (94%)
  local copies, waits for them, and re-layouts  5.67 us (5%)
    pallas_call x1, Pallas kernels, per_device(): pl.pallas_call(kernel, out_shape=(like((width, ff), BF), like((width, ff)...  118 us
    unnamed x11, local copies, waits for them, and re-layouts  4.91 us

profile of v4, /device:TPU:1, one launch (start us, length us, event | category | flops | bytes accessed | tf_op | source)
XLA Modules:
  0.0 124.0 jit_solution(16338350573872230935)
XLA Ops:
  0.6 0.0 copy-start.2
  0.6 0.0 copy-start.1
  0.7 0.0 copy-start
  0.7 0.7 copy-done.2
  1.3 0.0 copy-done.1
  1.3 0.0 copy-done
  1.4 117.7 %layer.1 = (bf16[2048,256]{1,0:T(8,128)(2,1)S(1)}, bf16[2048,256]{1,0:T(8,128)(2,1)S(1)}, bf16[256,2048]{1,0:T(8,128)(2,1)S(1)}, f32[32,256]{1,0:T(8,128)S(1)}, ...) custom-call(s32[2,256]{1,0:T(2,128)S(1)} %bitcast.17, f32[2,256]{1,0:T(2,128)S(1)} %bitcast.18, ...), custom_call_target="tpu_custom_call" | custom-call | tf_op jit(solution)/shard_map/layer/pallas_call | solution.py:494
  119.0 0.8 slice_bitcast_fusion
  119.8 1.0 copy.25
  120.7 1.0 copy.26
  121.7 1.0 copy.27
  122.7 0.6 copy.28
  123.3 0.7 copy.29
Async XLA Ops:
  0.6 0.7 copy-start.2
  0.6 0.7 copy-start.1
  0.7 0.7 copy-start

commit v5 on v4

--- a/solution.py
+++ b/solution.py
@@ -480,6 +480,33 @@
     for k in range(TP):
         to_partner(k).wait_send()
     wait_bytes(plane_in.at[pl.ds(0, PLANES - 1)], q_out)
+
+
+def store_kernel(*refs):
+    results, (small, *outs), sems = refs[:5], refs[5:-1], refs[-1]
+    sources = [*results, small.at[0], small.at[1], small.at[2]]
+    copies = [
+        pltpu.make_async_copy(a, b, sems.at[i]) for i, (a, b) in enumerate(zip(sources, outs, strict=True))
+    ]
+    for copy in copies:
+        copy.start()
+    for copy in copies:
+        copy.wait()
+
+
+def store(*results):
+    small = results[-1]
+    likes = [jax.ShapeDtypeStruct(a.shape, a.dtype) for a in results[:-1]]
+    likes += [jax.ShapeDtypeStruct(small.shape[1:], small.dtype)] * 3
+    return pl.pallas_call(
+        store_kernel,
+        out_shape=likes,
+        in_specs=[VMEM] * len(results),
+        out_specs=[pl.BlockSpec(memory_space=pltpu.HBM)] * len(likes),
+        scratch_shapes=[pltpu.SemaphoreType.DMA((len(likes),))],
+        compiler_params=pltpu.CompilerParams(vmem_limit_bytes=8 * 2**20),
+        name="store",
+    )(*results)
 
 
 def per_device(
@@ -569,9 +596,8 @@
             for v in (hidden_in, cotangent, w_gate[0], w_up[0], w_down[0], w_out, b_gate, c_gate, x_in)
         ],
     )
-    grad_gate, grad_up, grad_down, grad_out, residual, small = outs
-    grad_b, grad_c, grad_x = small[0], small[1], small[2]
-    return grad_gate[None], grad_up[None], grad_down[None], grad_out, residual, grad_b, grad_c, grad_x
+    grad_gate, grad_up, grad_down, *others = store(*outs)
+    return grad_gate[None], grad_up[None], grad_down[None], *others
 
 
 def solution(mesh):

time: 125 us -> 122 us (0.976)
  local copies, waits for them, and re-layouts: 5.67 us -> 0.69 us
  Pallas kernels: 118 us -> 120 us
    unnamed x11 -> x6, local copies, waits for them, and re-layouts: 4.91 us -> 0.69 us
    pallas_call x0 -> x1, Pallas kernels: none -> 1.95 us  [store(): pl.pallas_call(store_kernel, out_shape=likes, in_specs=[VMEM] * len(resul...]
where the time goes in v5:
time: 122 us; the launch traced here: 121 us
  Pallas kernels  120 us (98%)
    pallas_call x1, Pallas kernels, per_device(): pl.pallas_call(kernel, out_shape=(like((width, ff), BF), like((width, ff)...  118 us

profile of v5, /device:TPU:1, one launch (start us, length us, event | category | flops | bytes accessed | tf_op | source)
XLA Modules:
  0.0 121.0 jit_solution(9562124994017116335)
XLA Ops:
  0.6 0.0 copy-start.2
  0.6 0.0 copy-start.1
  0.7 0.0 copy-start
  0.7 0.7 copy-done.2
  1.3 0.0 copy-done.1
  1.3 0.0 copy-done
  1.4 117.7 %layer.1 = (bf16[2048,256]{1,0:T(8,128)(2,1)S(1)}, bf16[2048,256]{1,0:T(8,128)(2,1)S(1)}, bf16[256,2048]{1,0:T(8,128)(2,1)S(1)}, f32[32,256]{1,0:T(8,128)S(1)}, ...) custom-call(s32[2,256]{1,0:T(2,128)S(1)} %bitcast.8, f32[2,256]{1,0:T(2,128)S(1)} %bitcast.9, ...), custom_call_target="tpu_custom_call" | custom-call | tf_op jit(solution)/shard_map/layer/pallas_call | solution.py:521
  119.0 1.9 %store.1 = (bf16[2048,256]{1,0:T(8,128)(2,1)}, bf16[2048,256]{1,0:T(8,128)(2,1)}, bf16[256,2048]{1,0:T(8,128)(2,1)}, f32[32,256]{1,0:T(8,128)}, bf16[256,512]{1,...) custom-call(bf16[2048,256]{1,0:T(8,128)(2,1)S(1)} %get-tuple-element.22.refs_0_, ...), custom_call_target="tpu_custom_call" | custom-call | tf_op jit(solution)/shard_map/store/pallas_call | solution.py:501
Async XLA Ops:
  0.6 0.7 copy-start.2
  0.6 0.7 copy-start.1
  0.7 0.7 copy-start

commit v6 on v5

--- a/solution.py
+++ b/solution.py
@@ -26,6 +26,7 @@
 NEAR = (0, 6, 7)
 FAR = range(1, 6)
 NEAR_AT = 3
+FIRST = 4
 
 
 def plane_step(g):
@@ -52,9 +53,9 @@
 
 
 def kernel(
-    routes, weights, taps, hidden_hbm, cot_hbm, w_gate_hbm, w_up_hbm, w_down_hbm, w_out_hbm, b_hbm, c_hbm, x_hbm,
+    routes_hbm, weights_hbm, taps_hbm, hidden_hbm, cot_hbm, w_gate_hbm, w_up_hbm, w_down_hbm, w_out_hbm, b_hbm, c_hbm, x_hbm,
     grad_gate, grad_up, grad_down, grad_out, residual, small,
-    hidden, cot, w_gate, w_up, w_down, w_out, b_gate, c_gate, x_in,
+    routes, weights, taps, hidden, cot, w_gate, w_up, w_down, w_out, b_gate, c_gate, x_in,
     send, own, select, got, part, near_in, total_in, sums, back, d_both, hid_rows, full, y_short,
     edge, edge_in, outs, pair_in, pair_sum, outs_in, plane_sum, plane_in,
     ld, z_in, z_out, f_in, f_out, y_in, y_out, a_in, a_out, b_in, b_out, r_in, r_out,
@@ -72,11 +73,12 @@
     ff = w_gate.shape[1]
     out_rows = grad_out.shape[0]
 
-    barrier = greet_all(me, y, right, left)
     loads = [
         pltpu.make_async_copy(a, b, ld.at[i])
         for i, (a, b) in enumerate(
             (
+                (routes_hbm, routes),
+                (weights_hbm, weights),
                 (hidden_hbm, hidden),
                 (cot_hbm, cot),
                 (c_hbm, c_gate),
@@ -86,10 +88,14 @@
                 (w_down_hbm, w_down),
                 (b_hbm, b_gate),
                 (w_out_hbm, w_out),
+                (taps_hbm, taps),
             )
         )
     ]
-    for load in loads:
+    for load in loads[:FIRST]:
+        load.start()
+    barrier = greet_all(me, y, right, left)
+    for load in loads[FIRST:]:
         load.start()
 
     down = lax.broadcasted_iota(jnp.int32, (tokens, tokens), 0)
@@ -98,6 +104,8 @@
     def count(match):
         return jnp.sum(jnp.where(match, 1.0, 0.0), axis=0, keepdims=True).astype(jnp.int32)
 
+    loads[0].wait()
+    loads[1].wait()
     r0, r1 = routes[0:1, :], routes[1:2, :]
     w0, w1 = weights[0:1, :], weights[1:2, :]
     c0 = jnp.sum(jnp.where(down == across, r0, 0), axis=1, keepdims=True)
@@ -138,8 +146,8 @@
 
         lax.fori_loop(0, PLANE, one, 0)
 
-    loads[0].wait()
-    loads[1].wait()
+    loads[2].wait()
+    loads[3].wait()
     def pack_full(n):
         plane = plane_of(NEAR[n], 1)
         h, s, scale = picks(plane)
@@ -173,8 +181,8 @@
     pack_full(1)
     pack_full(2)
 
-    loads[2].wait()
-    loads[3].wait()
+    loads[4].wait()
+    loads[5].wait()
     edge[0] = c_gate[tokens - 8 :, :].astype(F32) * x_in[tokens - 8 :, :].astype(F32)
 
     def edge_copy(k, by):
@@ -183,7 +191,7 @@
         )
 
     edge_copy(0, 1).start()
-    for load in loads[4:7]:
+    for load in loads[6:9]:
         load.wait()
 
     def block(k, g, at=0, size=PLANE):
@@ -356,6 +364,7 @@
     for copy in sends:
         copy.start()
     t_row = lax.broadcasted_iota(jnp.int32, (tokens, 1), 0)
+    loads[11].wait()
     tap = [taps[i : i + 1, :].astype(F32) for i in range(3)]
     gated = c_gate[...].astype(F32) * x_in[...].astype(F32)
     edge_copy(0, 1).wait_recv()
@@ -365,10 +374,10 @@
         t_row == 0, before[6:7], jnp.where(t_row == 1, before[7:8], pltpu.roll(gated, 2, 0))
     )
     conv = tap[0] * two_back + tap[1] * one_back + tap[2] * gated
-    loads[7].wait()
+    loads[9].wait()
     b_f = b_gate[...].astype(F32)
     y_short[...] = (b_f * conv).astype(BF)
-    loads[8].wait()
+    loads[10].wait()
 
     def project(k):
         grad = dot(full[k], y_short[...], ((0,), (0,))).astype(BF)
@@ -528,9 +537,12 @@
             like((tokens, share), BF),
             like((3, tokens, short), BF),
         ),
-        in_specs=[VMEM] * 3 + [hbm] * 9,
+        in_specs=[hbm] * 12,
         out_specs=(VMEM,) * 6,
         scratch_shapes=[
+            pltpu.VMEM((2, tokens), jnp.int32),
+            pltpu.VMEM((2, tokens), F32),
+            pltpu.VMEM((3, short), BF),
             pltpu.VMEM((tokens, width), BF),
             pltpu.VMEM((tokens, width), BF),
             pltpu.VMEM((width, ff), BF),
@@ -561,7 +573,7 @@
             pltpu.VMEM((PLANE // 2, PLANES, out_rows, short), BF),
             pltpu.VMEM((PLANES, out_rows, short), BF),
             pltpu.VMEM((PLANES, out_rows, short), BF),
-            dma((9,)),
+            dma((12,)),
             dma((PLANES,)),
             dma(()),
             dma((len(NEAR),)),
@@ -590,10 +602,9 @@
         ),
         name="layer",
     )(
-        routes.T, routing_weights.T, taps,
         *[
             pltpu.with_memory_space_constraint(v, pltpu.HBM)
-            for v in (hidden_in, cotangent, w_gate[0], w_up[0], w_down[0], w_out, b_gate, c_gate, x_in)
+            for v in (routes.T, routing_weights.T, taps, hidden_in, cotangent, w_gate[0], w_up[0], w_down[0], w_out, b_gate, c_gate, x_in)
         ],
     )
     grad_gate, grad_up, grad_down, *others = store(*outs)

time: 122 us -> 121 us (level)
  no operation moved by 1% of the time
where the time goes in v6:
time: 121 us; the launch traced here: 120 us
  Pallas kernels  120 us (99%)
    pallas_call x1, Pallas kernels, per_device(): pl.pallas_call(kernel, out_shape=(like((width, ff), BF), like((width, ff)...  118 us

profile of v6, /device:TPU:1, one launch (start us, length us, event | category | flops | bytes accessed | tf_op | source)
XLA Modules:
  0.0 120.4 jit_solution(17172481850336363579)
XLA Ops:
  0.6 117.8 %layer.1 = (bf16[2048,256]{1,0:T(8,128)(2,1)S(1)}, bf16[2048,256]{1,0:T(8,128)(2,1)S(1)}, bf16[256,2048]{1,0:T(8,128)(2,1)S(1)}, f32[32,256]{1,0:T(8,128)S(1)}, ...) custom-call(s32[2,256]{1,0:T(2,128)} %bitcast.11, f32[2,256]{1,0:T(2,128)} %bitcast.12, ...), custom_call_target="tpu_custom_call" | custom-call | tf_op jit(solution)/shard_map/layer/pallas_call | solution.py:530
  118.5 1.9 %store.1 = (bf16[2048,256]{1,0:T(8,128)(2,1)}, bf16[2048,256]{1,0:T(8,128)(2,1)}, bf16[256,2048]{1,0:T(8,128)(2,1)}, f32[32,256]{1,0:T(8,128)}, bf16[256,512]{1,...) custom-call(bf16[2048,256]{1,0:T(8,128)(2,1)S(1)} %get-tuple-element.22.refs_0_, ...), custom_call_target="tpu_custom_call" | custom-call | tf_op jit(solution)/shard_map/store/pallas_call | solution.py:510
